TPU v7x, 256 devices: a whole 4x4x8 slice. The times are simulated.
256 devices in a mesh: ep: 16 (over y, x), tp: 16 (over z, core).
Axes of the slice: x: 4, y: 4, z: 8, core: 2. Of those that a mesh axis runs over, the one named last changes fastest.
Arguments:
- tokens: bfloat16 [1024, 2048], P('ep', 'tp'), may hold values from -6 to 6
- conv_state: bfloat16 [1024, 3, 2048], P('ep', None, 'tp'), may hold values from -6 to 6
- recur_state: float32 [1024, 2048], P('ep', 'tp'), may hold values from -6 to 6
- norm1_gain: bfloat16 [2048], P('tp'), may hold values from 0.099609375 to 1.8984375
- branch_weight: bfloat16 [2048, 2048], P(None, 'tp'), may hold values from -0.125 to 0.125
- gating_weight: bfloat16 [2048, 2048], P(None, 'tp'), may hold values from -0.125 to 0.125
- conv_taps: bfloat16 [4, 2048], P(None, 'tp'), may hold values from -3 to 3
- conv_bias: bfloat16 [2048], P('tp'), may hold values from -3 to 3
- recur_weight: bfloat16 [16, 128, 128], P('tp'), may hold values from -0.5 to 0.5
- recur_bias: float32 [2048], P('tp'), may hold values from -4 to 4
- input_weight: bfloat16 [16, 128, 128], P('tp'), may hold values from -0.5 to 0.5
- input_bias: float32 [2048], P('tp'), may hold values from -4 to 4
- decay_logit: float32 [2048], P('tp'), may hold values from 1.5 to 7.5
- out_weight: bfloat16 [2048, 2048], P(None, 'tp'), may hold values from -0.125 to 0.125
- norm2_gain: bfloat16 [2048], P('tp'), may hold values from 0.099609375 to 1.8984375
- group_router: bfloat16 [2048, 4], replicated, may hold values from -0.125 to 0.125
- expert_router: bfloat16 [2048, 16], replicated, may hold values from -0.125 to 0.125
- routes: int32 [1024, 2], P('ep'), may hold values from 0 to 15, as said below
- gate_experts: bfloat16 [16, 2048, 1024], P('ep', None, 'tp'), may hold values from -0.125 to 0.125
- up_experts: bfloat16 [16, 2048, 1024], P('ep', None, 'tp'), may hold values from -0.125 to 0.125
- down_experts: bfloat16 [16, 1024, 2048], P('ep', 'tp'), may hold values from -0.75 to 0.75
Outputs:
- mixed: bfloat16 [1024, 2048], P('ep', 'tp')
- new_state: float32 [1024, 2048], P('ep', 'tp')
- new_conv: bfloat16 [1024, 3, 2048], P('ep', None, 'tp')
Inputs may be any that keep to these rules, and one draw needn't show every extreme that they name: `routes`: each row names 2 different experts. In each aligned block of 64 rows (the rows of one index of ep) exactly half of the 16 experts are named, each by exactly 16 rows, and some expert is named by 16 rows in every block.
All inputs are finite; a program needn't handle non-finite values.
Results may differ from a plain program's by a relative error of at most 0.018.
Values may be sent and summed in bfloat16 or wider, within the bound.
A program may use at most 64 MiB of HBM per device.

v0:
```python
import jax
import jax.numpy as jnp
from jax import lax
from jax.sharding import PartitionSpec as P

EPS = 1e-06


def from_everyone(array, axis):
    count = lax.axis_size(axis)
    return lax.all_to_all(
        jnp.broadcast_to(array[None], (count, *array.shape)), axis, 0, 0, tiled=True
    )


def taken_together(array, axis):
    return from_everyone(array, axis).sum(axis=0)


def laid_out(blocks, dim):
    blocks = jnp.moveaxis(blocks, 0, dim)
    dims = blocks.shape
    return blocks.reshape(*dims[:dim], dims[dim] * dims[dim + 1], *dims[dim + 2 :])


def gathered_copies(array, axis, dim):
    return laid_out(from_everyone(array, axis), dim)


def split_up(array, dim, count):
    dims = array.shape
    blocks = array.reshape(*dims[:dim], count, dims[dim] // count, *dims[dim + 1 :])
    return jnp.moveaxis(blocks, dim, 0)


def sent_and_summed(array, axis, dim):
    count = lax.axis_size(axis)
    blocks = lax.all_to_all(split_up(array, dim, count), axis, 0, 0, tiled=True)
    return jnp.sum(blocks.astype(jnp.float32), axis=0)


def second_scale(resid_float, width):
    squares_two = taken_together(jnp.sum(resid_float * resid_float, axis=1), "tp")
    return lax.rsqrt(squares_two / width + EPS)[:, None]


def on_device(
    tokens,
    conv_state,
    recur_state,
    norm1_gain,
    branch_weight,
    gating_weight,
    conv_taps,
    conv_bias,
    recur_weight,
    recur_bias,
    input_weight,
    input_bias,
    decay_logit,
    out_weight,
    norm2_gain,
    group_router,
    expert_router,
    routes,
    gate_experts,
    up_experts,
    down_experts,
):
    seqs = tokens.shape[0]
    feat_local = tokens.shape[1]
    width = feat_local * lax.axis_size("tp")
    channels = branch_weight.shape[1]
    tok_float = tokens.astype(jnp.float32)
    own_squares = jnp.sum(tok_float * tok_float, axis=1)
    squares = taken_together(own_squares, "tp")
    rstd_one = lax.rsqrt(squares / width + EPS)[:, None]
    normed = (tok_float * rstd_one * norm1_gain.astype(jnp.float32)).astype(jnp.bfloat16)
    piece = gathered_copies(normed, "tp", 1)
    branch_float = jnp.dot(piece, branch_weight, preferred_element_type=jnp.float32)
    gating_float = jnp.dot(piece, gating_weight, preferred_element_type=jnp.float32)
    branch = branch_float.astype(jnp.bfloat16)
    gating = gating_float.astype(jnp.bfloat16)
    window = jnp.concatenate([conv_state, branch[:, None, :]], axis=1)
    new_conv = window[:, 1:]
    conv_out = conv_bias.astype(jnp.float32) + jnp.sum(
        conv_taps.astype(jnp.float32)[None] * window.astype(jnp.float32), axis=1
    )
    conv_low = conv_out.astype(jnp.bfloat16)
    blocks = conv_low.reshape(seqs, recur_weight.shape[0], recur_weight.shape[1])
    recur_gate = jax.nn.sigmoid(
        jnp.einsum(
            "bnc,ncd->bnd", blocks, recur_weight, preferred_element_type=jnp.float32
        ).reshape(seqs, channels)
        + recur_bias
    )
    input_gate = jax.nn.sigmoid(
        jnp.einsum(
            "bnc,ncd->bnd", blocks, input_weight, preferred_element_type=jnp.float32
        ).reshape(seqs, channels)
        + input_bias
    )
    log_decay = 8.0 * recur_gate * jax.nn.log_sigmoid(decay_logit)
    new_state = jnp.exp(log_decay) * recur_state + jnp.sqrt(-jnp.expm1(2.0 * log_decay)) * (
        input_gate * conv_out
    )
    hidden_mix = (new_state * jax.nn.gelu(gating.astype(jnp.float32))).astype(jnp.bfloat16)
    mixer_out = jnp.dot(
        gathered_copies(hidden_mix, "tp", 1), out_weight, preferred_element_type=jnp.float32
    )
    resid = (tok_float + mixer_out).astype(jnp.bfloat16)
    resid_float = resid.astype(jnp.float32)
    gain_two = norm2_gain.astype(jnp.float32)
    normed2 = (resid_float * second_scale(resid_float, width) * gain_two).astype(jnp.bfloat16)
    full_rows = gathered_copies(normed2, "tp", 1)
    group_logits = jnp.dot(full_rows, group_router, preferred_element_type=jnp.float32)
    expert_logits = jnp.dot(full_rows, expert_router, preferred_element_type=jnp.float32)
    experts_total = expert_router.shape[1]
    groups_total = group_router.shape[1]
    group_size = experts_total // groups_total
    top_count = routes.shape[1]
    capacity = 2 * top_count * seqs // experts_total
    group_exp = jnp.exp(group_logits)
    group_prob = group_exp / jnp.sum(group_exp, axis=-1, keepdims=True)
    expert_ids = jnp.arange(experts_total, dtype=jnp.int32)
    chosen = (routes[..., None] == expert_ids).astype(jnp.float32)
    chosen_logit = jnp.sum(chosen * expert_logits[:, None, :], axis=-1)
    pair_exp = jnp.exp(chosen_logit)
    share = pair_exp / jnp.sum(pair_exp, axis=-1, keepdims=True)
    group_ids = jnp.arange(groups_total, dtype=jnp.int32)
    group_hit = ((routes // group_size)[..., None] == group_ids).astype(jnp.float32)
    route_weight = jnp.sum(group_hit * group_prob[:, None, :], axis=-1) * share
    flat = routes.reshape(-1)
    hits = (flat[:, None] == expert_ids[None, :]).astype(jnp.int32)
    rank = jnp.sum((jnp.cumsum(hits, axis=0) - hits) * hits, axis=1)
    slot = flat * capacity + rank
    slot_ids = jnp.arange(experts_total * capacity, dtype=jnp.int32)
    slot_hits = (
        (slot[:, None] == slot_ids[None, :]).astype(jnp.float32).reshape(seqs, top_count, -1)
    )
    selection = jnp.sum(slot_hits, axis=1).astype(jnp.bfloat16)
    combine = jnp.sum(route_weight[..., None] * slot_hits, axis=1)
    send = jnp.einsum("sc,sd->cd", selection, full_rows, preferred_element_type=jnp.float32).astype(
        jnp.bfloat16
    )
    exp_local = gate_experts.shape[0]
    send = send.reshape(lax.axis_size("ep"), exp_local, capacity, full_rows.shape[1])
    arrived = lax.all_to_all(send, "ep", split_axis=0, concat_axis=0, tiled=True)
    gate = jnp.einsum("sacd,adf->sacf", arrived, gate_experts, preferred_element_type=jnp.float32)
    upper = jnp.einsum("sacd,adf->sacf", arrived, up_experts, preferred_element_type=jnp.float32)
    hidden = (jax.nn.silu(gate) * upper).astype(jnp.bfloat16)
    partial_out = jnp.einsum(
        "sacf,afd->sacd", hidden, down_experts, preferred_element_type=jnp.float32
    )
    summed = sent_and_summed(partial_out.astype(jnp.bfloat16), "tp", 3).astype(jnp.bfloat16)
    back = lax.all_to_all(summed, "ep", split_axis=0, concat_axis=0, tiled=True)
    back = back.reshape(experts_total * capacity, feat_local).astype(jnp.float32)
    moe = jnp.dot(combine, back, precision=lax.Precision.HIGHEST)
    mixed = (resid_float + moe).astype(jnp.bfloat16)
    return (mixed, new_state, new_conv)


def solution(mesh):
    return jax.shard_map(
        on_device,
        mesh=mesh,
        in_specs=(
            P("ep", "tp"),
            P("ep", None, "tp"),
            P("ep", "tp"),
            P("tp"),
            P(None, "tp"),
            P(None, "tp"),
            P(None, "tp"),
            P("tp"),
            P("tp", None, None),
            P("tp"),
            P("tp", None, None),
            P("tp"),
            P("tp"),
            P(None, "tp"),
            P("tp"),
            P(),
            P(),
            P("ep", None),
            P("ep", None, "tp"),
            P("ep", None, "tp"),
            P("ep", "tp", None),
        ),
        out_specs=(P("ep", "tp"), P("ep", "tp"), P("ep", None, "tp")),
        check_vma=False,
    )
```

profile of v0, /device:TPU:1, one launch (start us, length us, event | category | flops | bytes accessed | tf_op | source)
XLA Modules:
  0.0 151.6 jit_solution(17607228275012154630)
XLA Ops:
  0.7 0.9 fusion.50
  1.6 0.6 broadcast_in_dim.12
  2.2 10.0 %all-to-all-start = ((f32[16,1,64]{2,1,0:T(1,128)}), f32[16,1,64]{2,1,0:T(1,128)S(1)}, u32[]{:S(2)}, u32[]{:S(2)}) async-start(f32[16,1,64]{2,1,0:T(1,128)} %broadcast_in_dim.12), calls=%async_computation | async-start | bytes 16384 | tf_op jit(solution)/shard_map/all_to_all | solution.py:11
  12.2 0.7 convert_element_type.106
  12.9 6.3 %all-to-all-done = f32[16,1,64]{2,1,0:T(1,128)S(1)} async-done(((f32[16,1,64]{2,1,0:T(1,128)}), f32[16,1,64]{2,1,0:T(1,128)S(1)}, u32[]{:S(2)}, u32[]{:S(2)}) %all-to-all-start) | async-done | bytes 4128 | tf_op jit(solution)/shard_map/all_to_all | solution.py:11
  19.2 0.8 fusion.52
  20.0 0.7 broadcast_in_dim.13
  20.7 4.0 %all-to-all-start.1 = ((bf16[16,64,128]{2,1,0:T(8,128)(2,1)}), bf16[16,64,128]{2,1,0:T(8,128)(2,1)S(1)}, u32[]{:S(2)}, u32[]{:S(2)}) async-start(bf16[16,64,128]{2,1,0:T(8,128)(2,1)} %broadcast_in_dim.13), calls=%async_computation.1 | async-start | bytes 524288 | tf_op jit(solution)/shard_map/all_to_all | solution.py:11
  24.7 0.7 convert_element_type.105
  25.4 0.7 convert_element_type.104
  26.1 0.7 fusion.78
  26.7 9.7 %all-to-all-done.1 = bf16[16,64,128]{2,1,0:T(8,128)(2,1)S(1)} async-done(((bf16[16,64,128]{2,1,0:T(8,128)(2,1)}), bf16[16,64,128]{2,1,0:T(8,128)(2,1)S(1)}, u32[]{:S(2)}, u32[]{:S(2)}) %all-to-all-start.1) | async-done | bytes 262176 | tf_op jit(solution)/shard_map/all_to_all | solution.py:11
  36.5 1.3 fusion.20
  37.8 0.1 fusion.15
  38.0 0.2 fusion.10
  38.2 0.2 fusion.65
  38.5 14.2 %all_to_all.42 = bf16[16,64,128]{2,1,0:T(8,128)(2,1)S(1)} all-to-all(bf16[16,64,128]{2,1,0:T(8,128)(2,1)S(1)} %broadcast_in_dim.15), channel_id=1, replica_groups=mesh['ep'=16,'tp'=16] {'tp'}, dimensions={0} | all-to-all | bytes 524288 | tf_op jit(solution)/shard_map/all_to_all | solution.py:11
  52.7 0.3 multiply_reduce_fusion.1
  53.1 0.6 broadcast_in_dim.16
  53.7 3.4 %all-to-all-start.3 = ((f32[16,1,64]{2,1,0:T(1,128)}), f32[16,1,64]{2,1,0:T(1,128)S(1)}, u32[]{:S(2)}, u32[]{:S(2)}) async-start(f32[16,1,64]{2,1,0:T(1,128)} %broadcast_in_dim.16), calls=%async_computation.3 | async-start | bytes 16384 | tf_op jit(solution)/shard_map/all_to_all | solution.py:11
  57.1 0.1 copy.73
  57.2 0.1 eq.27
  57.3 6.3 %all-to-all-done.3 = f32[16,1,64]{2,1,0:T(1,128)S(1)} async-done(((f32[16,1,64]{2,1,0:T(1,128)}), f32[16,1,64]{2,1,0:T(1,128)S(1)}, u32[]{:S(2)}, u32[]{:S(2)}) %all-to-all-start.3) | async-done | bytes 4128 | tf_op jit(solution)/shard_map/all_to_all | solution.py:11
  63.7 0.1 multiply_convert_fusion
  63.8 0.8 broadcast_in_dim.17
  64.5 4.0 %all-to-all-start.4 = ((bf16[16,64,128]{2,1,0:T(8,128)(2,1)}), bf16[16,64,128]{2,1,0:T(8,128)(2,1)S(1)}, u32[]{:S(2)}, u32[]{:S(2)}) async-start(bf16[16,64,128]{2,1,0:T(8,128)(2,1)} %broadcast_in_dim.17), calls=%async_computation.4 | async-start | bytes 524288 | tf_op jit(solution)/shard_map/all_to_all | solution.py:11
  68.5 0.1 fusion.48
  68.6 0.2 reduce_window_sum.11
  68.7 0.2 select_reduce_fusion.1
  68.9 0.1 reduce_sum.131
  69.1 0.1 copy.74
  69.2 11.1 %all-to-all-done.4 = bf16[16,64,128]{2,1,0:T(8,128)(2,1)S(1)} async-done(((bf16[16,64,128]{2,1,0:T(8,128)(2,1)}), bf16[16,64,128]{2,1,0:T(8,128)(2,1)S(1)}, u32[]{:S(2)}, u32[]{:S(2)}) %all-to-all-start.4) | async-done | bytes 262176 | tf_op jit(solution)/shard_map/all_to_all | solution.py:11
  80.2 0.2 fusion.26
  80.5 0.2 fusion.80
  80.7 0.1 convert_reduce_fusion
  80.8 0.5 convolution_convert_fusion.1
  81.3 24.7 %all_to_all.43 = bf16[16,1,16,2048]{3,2,1,0:T(8,128)(2,1)S(1)} all-to-all(bf16[16,1,16,2048]{3,2,1,0:T(8,128)(2,1)S(1)} %bitcast.141), channel_id=1, replica_groups=mesh['ep'=16,'tp'=16] {'ep'}, dimensions={0} | all-to-all | bytes 2097152 | tf_op jit(solution)/shard_map/all_to_all | solution.py:148
  106.0 0.4 convolution_bitcast_fusion.1
  106.4 0.5 copy-done.3
  106.9 0.1 copy-done.4
  107.0 1.3 fusion
  108.3 0.3 copy.118
  108.6 31.6 %all_to_all.44 = bf16[16,16,1,16,128]{4,3,1,2,0:T(8,128)(2,1)S(1)} all-to-all(bf16[16,16,1,16,128]{4,3,1,2,0:T(8,128)(2,1)S(1)} %bitcast.142), channel_id=1, replica_groups=mesh['ep'=16,'tp'=16] {'tp'}, dimensions={0} | all-to-all | bytes 2097152 | tf_op jit(solution)/shard_map/all_to_all | solution.py:38
  140.1 0.8 reduce_sum.140
  140.9 3.5 %all-to-all-start.7 = ((bf16[16,1,16,128]{3,2,1,0:T(8,128)(2,1)}), bf16[16,1,16,128]{3,2,1,0:T(8,128)(2,1)S(1)}, u32[]{:S(2)}, u32[]{:S(2)}) async-start(bf16[16,1,16,128]{3,2,1,0:T(8,128)(2,1)} %bitcast.32), calls=%async_computation.7 | async-start | bytes 131072 | tf_op jit(solution)/shard_map/all_to_all | solution.py:156
  144.4 0.6 fusion.49
  145.0 5.8 %all-to-all-done.7 = bf16[16,1,16,128]{3,2,1,0:T(8,128)(2,1)S(1)} async-done(((bf16[16,1,16,128]{3,2,1,0:T(8,128)(2,1)}), bf16[16,1,16,128]{3,2,1,0:T(8,128)(2,1)S(1)}, u32[]{:S(2)}, u32[]{:S(2)}) %all-to-all-start.7) | async-done | bytes 65568 | tf_op jit(solution)/shard_map/all_to_all | solution.py:156
  150.8 0.8 fusion.18
  (45 shorter events, 0.3 us)
Async XLA Ops:
  0.6 52.1 %copy-start = (bf16[2048,128]{1,0:T(8,128)(2,1)S(1)}, bf16[2048,128]{1,0:T(8,128)(2,1)}, u32[]{:S(2)}) copy-start(bf16[2048,128]{1,0:T(8,128)(2,1)} %param.34) | copy-start | bytes 1572868
  0.6 37.1 %copy-start.5 = (bf16[64,3,128]{2,0,1:T(8,128)(2,1)S(1)}, bf16[64,3,128]{2,0,1:T(8,128)(2,1)}, u32[]{:S(2)}) copy-start(bf16[64,3,128]{2,0,1:T(8,128)(2,1)} %param.22) | copy-start | bytes 147460
  0.7 37.1 %copy-start.10 = (bf16[1,128,128]{2,1,0:T(8,128)(2,1)S(1)}, bf16[1,128,128]{2,1,0:T(8,128)(2,1)}, u32[]{:S(2)}) copy-start(bf16[1,128,128]{2,1,0:T(8,128)(2,1)} %param.29) | copy-start | bytes 98308
  0.7 37.1 %copy-start.14 = (f32[128]{0:T(128)S(1)}, f32[128]{0:T(128)}, u32[]{:S(2)}) copy-start(f32[128]{0:T(128)} %param.30) | copy-start | bytes 1540
  0.7 37.3 %copy-start.11 = (bf16[1,128,128]{2,1,0:T(8,128)(2,1)S(1)}, bf16[1,128,128]{2,1,0:T(8,128)(2,1)}, u32[]{:S(2)}) copy-start(bf16[1,128,128]{2,1,0:T(8,128)(2,1)} %param.31) | copy-start | bytes 98308
  0.7 37.3 %copy-start.12 = (f32[64,128]{1,0:T(8,128)S(1)}, f32[64,128]{1,0:T(8,128)}, u32[]{:S(2)}) copy-start(f32[64,128]{1,0:T(8,128)} %param.23) | copy-start | bytes 98308
  0.7 37.3 %copy-start.15 = (f32[128]{0:T(128)S(1)}, f32[128]{0:T(128)}, u32[]{:S(2)}) copy-start(f32[128]{0:T(128)} %param.32) | copy-start | bytes 1540
  2.2 16.9 %all-to-all-start = ((f32[16,1,64]{2,1,0:T(1,128)}), f32[16,1,64]{2,1,0:T(1,128)S(1)}, u32[]{:S(2)}, u32[]{:S(2)}) async-start(f32[16,1,64]{2,1,0:T(1,128)} %broadcast_in_dim.12), calls=%async_computation | async-start | bytes 16384 | tf_op jit(solution)/shard_map/all_to_all | solution.py:11
  20.0 18.2 %copy-start.1 = (bf16[2048,128]{1,0:T(8,128)(2,1)S(1)}, bf16[2048,128]{1,0:T(8,128)(2,1)}, u32[]{:S(2)}) copy-start(bf16[2048,128]{1,0:T(8,128)(2,1)} %param.26) | copy-start | bytes 1572868
  20.7 15.7 %all-to-all-start.1 = ((bf16[16,64,128]{2,1,0:T(8,128)(2,1)}), bf16[16,64,128]{2,1,0:T(8,128)(2,1)S(1)}, u32[]{:S(2)}, u32[]{:S(2)}) async-start(bf16[16,64,128]{2,1,0:T(8,128)(2,1)} %broadcast_in_dim.13), calls=%async_computation.1 | async-start | bytes 524288 | tf_op jit(solution)/shard_map/all_to_all | solution.py:11
  37.8 14.9 %copy-start.6 = (bf16[64,128]{1,0:T(8,128)(2,1)S(1)}, bf16[64,128]{1,0:T(8,128)(2,1)}, u32[]{:S(2)}) copy-start(bf16[64,128]{1,0:T(8,128)(2,1)} %param.21) | copy-start | bytes 49156
  38.2 14.9 %copy-start.7 = (f32[64,128]{1,0:T(8,128)}, f32[64,128]{1,0:T(8,128)S(1)}, u32[]{:S(2)}) copy-start(f32[64,128]{1,0:T(8,128)S(1)} %fusion.10) | copy-start | bytes 98308
  38.2 18.9 %copy-start.8 = (s32[64,2]{0,1:T(2,128)S(1)}, s32[64,2]{0,1:T(2,128)}, u32[]{:S(2)}) copy-start(s32[64,2]{0,1:T(2,128)} %param.38) | copy-start | bytes 1540
  38.4 18.9 %copy-start.16 = (bf16[128]{0:T(256)(128)(2,1)S(1)}, bf16[128]{0:T(256)(128)(2,1)}, u32[]{:S(2)}) copy-start(bf16[128]{0:T(256)(128)(2,1)} %param.35) | copy-start | bytes 772
  52.7 27.5 %copy-start.9 = (bf16[2048,16]{0,1:T(8,128)(2,1)S(1)}, bf16[2048,16]{0,1:T(8,128)(2,1)}, u32[]{:S(2)}) copy-start(bf16[2048,16]{0,1:T(8,128)(2,1)} %param.37) | copy-start | bytes 196612
  53.1 27.4 %copy-start.13 = (bf16[2048,4]{0,1:T(4,128)(2,1)S(1)}, bf16[2048,4]{0,1:T(4,128)(2,1)}, u32[]{:S(2)}) copy-start(bf16[2048,4]{0,1:T(4,128)(2,1)} %param.36) | copy-start | bytes 49156
  53.7 10.0 %all-to-all-start.3 = ((f32[16,1,64]{2,1,0:T(1,128)}), f32[16,1,64]{2,1,0:T(1,128)S(1)}, u32[]{:S(2)}, u32[]{:S(2)}) async-start(f32[16,1,64]{2,1,0:T(1,128)} %broadcast_in_dim.16), calls=%async_computation.3 | async-start | bytes 16384 | tf_op jit(solution)/shard_map/all_to_all | solution.py:11
  64.5 15.7 %all-to-all-start.4 = ((bf16[16,64,128]{2,1,0:T(8,128)(2,1)}), bf16[16,64,128]{2,1,0:T(8,128)(2,1)S(1)}, u32[]{:S(2)}, u32[]{:S(2)}) async-start(bf16[16,64,128]{2,1,0:T(8,128)(2,1)} %broadcast_in_dim.17), calls=%async_computation.4 | async-start | bytes 524288 | tf_op jit(solution)/shard_map/all_to_all | solution.py:11
  81.3 24.7 %copy-start.2 = (bf16[1,2048,64]{1,2,0:T(8,128)(2,1)S(1)}, bf16[1,2048,64]{1,2,0:T(8,128)(2,1)}, u32[]{:S(2)}) copy-start(bf16[1,2048,64]{1,2,0:T(8,128)(2,1)} %param.39) | copy-start | bytes 786436
  106.0 1.0 copy-start.3
  106.0 1.0 copy-start.4
  140.9 10.0 %all-to-all-start.7 = ((bf16[16,1,16,128]{3,2,1,0:T(8,128)(2,1)}), bf16[16,1,16,128]{3,2,1,0:T(8,128)(2,1)S(1)}, u32[]{:S(2)}, u32[]{:S(2)}) async-start(bf16[16,1,16,128]{3,2,1,0:T(8,128)(2,1)} %bitcast.32), calls=%async_computation.7 | async-start | bytes 131072 | tf_op jit(solution)/shard_map/all_to_all | solution.py:156
where the time goes:
time: 152 us
  blocking collectives  70.5 us (46%)
  waiting for transfers between devices  39.3 us (26%)
  starting transfers between devices  24.8 us (16%)
  other arithmetic  6.55 us (4%)
  matrix products  5.39 us (4%)
  local copies, waits for them, and re-layouts  4.15 us (3%)
    all_to_all x4, waiting for transfers between devices, from_everyone(): lax.all_to_all(jnp.broadcast_to(array[None], (count, *array.shape)), axis...  33.4 us
    all_to_all x1, blocking collectives, sent_and_summed(): blocks = lax.all_to_all(split_up(array, dim, count), axis, 0, 0, tiled=True)  31.6 us
    all_to_all x1, blocking collectives, on_device(): lax.all_to_all(send, 'ep', split_axis=0, concat_axis=0, tiled=True)  24.7 us
    all_to_all x4, starting transfers between devices, from_everyone(): lax.all_to_all(jnp.broadcast_to(array[None], (count, *array.shape)), axis...  21.3 us
    all_to_all x1, blocking collectives, from_everyone(): lax.all_to_all(jnp.broadcast_to(array[None], (count, *array.shape)), axis...  14.2 us
    all_to_all x1, waiting for transfers between devices, on_device(): back = lax.all_to_all(summed, 'ep', split_axis=0, concat_axis=0, tiled=True)  5.83 us
    all_to_all x1, starting transfers between devices, on_device(): back = lax.all_to_all(summed, 'ep', split_axis=0, concat_axis=0, tiled=True)  3.5 us
  transfers between devices with their start and end apart: 5, of which 5 were waited for; matrix products, arithmetic and copies ran while one was open for 3% of the time, Pallas kernels for 0%

commit v1 on v0

v1 whole, which is shorter than its diff:
```python
import functools

import jax
import jax.numpy as jnp
from jax import lax
from jax.experimental import pallas as pl
from jax.experimental.pallas import tpu as pltpu
from jax.sharding import PartitionSpec as P

EPS = 1e-06
F32 = jnp.float32
BF16 = jnp.bfloat16
MESH = pl.DeviceIdType.MESH
NT = (((1,), (1,)), ((), ()))


def mm(a, b):
    return jnp.dot(a, b, preferred_element_type=F32)


def mm_nt(a, b):
    return lax.dot_general(a, b, NT, preferred_element_type=F32)


def expm1_neg(x):
    series = x * (1.0 + x * (0.5 + x * (1.0 / 6 + x * (1.0 / 24 + x * (1.0 / 120 + x / 720)))))
    return jnp.where(x > -0.2, -series, 1.0 - jnp.exp(x))


def log_sigmoid(x):
    u = jnp.exp(-jnp.abs(x))
    w = u / (2.0 + u)
    w2 = w * w
    poly = 1.0 / 15
    for k in (13, 11, 9, 7, 5, 3, 1):
        poly = poly * w2 + 1.0 / k
    return jnp.minimum(x, 0.0) - 2.0 * w * poly


def gelu(x):
    return 0.5 * x * (1.0 + jnp.tanh(0.7978845608028654 * (x + 0.044715 * x * x * x)))


def sigmoid(x):
    return 1.0 / (1.0 + jnp.exp(-x))


def kernel(
    EP, NZ, S, CAP, GS,
    tok_h, conv_h, state_h, par_h, bw_h, gw_h, rw_h, iw_h, ow_h, grt_h, ert_h, rt_h, gt_h, ut_h, dn_h,
    mixed_h, nstate_h, nconv_h,
    tok_a, gain_a, conv_v, state_v, par_v, bw_v, gw_v, rw_v, iw_v, ow_v, grt_v, ert_v, rt_v, wcat, wdn,
    hid_b, res_c, ysel, xbuf, rexp, lg_own, lg_in, ss_own, ss_in, acc_v, pacc_v, ssx_v, pss_v,
    hid_e, y_v, back_v, mixed_v, nstate_v, branch_v, sel_v, selt_v,
    sem_ld, s_a, r_a, f_a, s_g, r_g, f_g, s_b, r_b, f_b, s_w, r_w, f_w, s_x, r_x,
    s_c, r_c, s_d, r_d, s_l, r_l, s_p, r_p, s_e, r_e, s_f, r_f, sem_o,
):
    me = lax.axis_index("ep")
    tp = lax.axis_index("tp")
    z = tp // 2
    c = tp % 2
    L = EP * CAP
    HALF = L // 2
    HS = EP // 2
    WIDTH = NZ * 256
    other = 1 - c
    partner = (me, 2 * z + other)

    def zdev(d):
        return (me, 2 * ((z + d) % NZ) + c)

    def zrel(rd):
        return (z + rd) % NZ

    def rows(j, rd):
        t = 2 * zrel(rd) + (c if j == 0 else other)
        return pl.multiple_of(t * 128, 128)

    def back_rel(d):
        return (NZ - d) % NZ

    far_first = sorted(range(1, NZ), key=lambda d: (-min(d, NZ - d), d))
    near_first = [0] + sorted(range(1, NZ), key=lambda d: (min(d, NZ - d), d))

    def wait(ref, sem):
        pltpu.make_async_copy(ref, ref, sem).wait()

    def send(src, dst, ssem, rsem, dev):
        pltpu.make_async_remote_copy(
            src_ref=src, dst_ref=dst, send_sem=ssem, recv_sem=rsem, device_id=dev, device_id_type=MESH
        ).start()

    loads = []

    def load(src, dst):
        k = len(loads)
        cp = pltpu.make_async_copy(src, dst, sem_ld.at[k])
        cp.start()
        loads.append(cp)
        return k

    k_tok = load(tok_h, tok_a.at[0, 0])
    k_par = load(par_h, par_v)
    k_rt = load(rt_h, rt_v)

    bar = pltpu.get_barrier_semaphore()

    def sig(dev):
        pl.semaphore_signal(bar, inc=1, device_id=dev, device_id_type=MESH)

    for d in range(1, NZ):
        sig(zdev(d))
    sig(partner)

    def bar_ep(i, carry):
        e = (me + i) % EP
        sig((e, tp))
        sig((e, 2 * z + other))
        return carry

    lax.fori_loop(1, EP, bar_ep, 0)

    k_conv = load(conv_h, conv_v)
    k_state = load(state_h, state_v)
    k_bw = load(bw_h, bw_v)
    k_gw = load(gw_h, gw_v)
    k_rw = load(rw_h, rw_v)
    k_iw = load(iw_h, iw_v)
    k_ow = load(ow_h, ow_v)
    k_gr = load(grt_h, grt_v)
    k_er = load(ert_h, ert_v)
    k_w = [load(dn_h.at[:, pl.ds(pl.multiple_of(z * 256, 256), 256)], wdn.at[0, 0])]
    k_x = []
    for rd in range(NZ):
        cols = pl.ds(rows(0, rd), 128)
        k_x.append(load(gt_h.at[:, cols], wcat.at[rd, 0]))
        k_x.append(load(ut_h.at[:, cols], wcat.at[rd, 2]))

    loads[k_tok].wait()
    loads[k_par].wait()
    gain_a[0, 0] = par_v[0:2, :]

    pl.semaphore_wait(bar, (NZ - 1) + 1 + 2 * (EP - 1))

    for d in far_first:
        rd = back_rel(d)
        send(gain_a.at[0, 0], gain_a.at[rd, 0], s_g.at[d], r_g.at[rd, 0], zdev(d))
        send(tok_a.at[0, 0], tok_a.at[rd, 0], s_a.at[d], r_a.at[rd, 0], zdev(d))
    send(gain_a.at[0, 0], gain_a.at[0, 1], f_g.at[0], r_g.at[0, 1], partner)
    send(tok_a.at[0, 0], tok_a.at[0, 1], f_a.at[0], r_a.at[0, 1], partner)

    for d in far_first:
        cols = pl.ds(pl.multiple_of(((z + d) % NZ) * 256, 256), 256)
        rd = back_rel(d)
        send(dn_h.at[:, cols], wdn.at[rd, 0], s_w.at[d], r_w.at[rd, 0], zdev(d))
    for rd in range(NZ):
        cols = pl.ds(rows(1, rd), 128)
        send(gt_h.at[:, cols], wcat.at[rd, 1], s_x.at[rd, 0], r_x.at[rd, 0], partner)
        send(ut_h.at[:, cols], wcat.at[rd, 3], s_x.at[rd, 1], r_x.at[rd, 1], partner)

    loads[k_rt].wait()
    loads[k_gr].wait()
    loads[k_er].wait()
    slot_row = lax.broadcasted_iota(jnp.int32, (L, S), 0)
    r0 = rt_v[0:1, :]
    r1 = rt_v[1:2, :]
    hit = ((slot_row // CAP) == r0) | ((slot_row // CAP) == r1)
    hit_f = jnp.where(hit, 1.0, 0.0)
    hit_b = hit_f.astype(BF16)
    before = jnp.where(
        lax.broadcasted_iota(jnp.int32, (S, S), 0) < lax.broadcasted_iota(jnp.int32, (S, S), 1), 1.0, 0.0
    ).astype(BF16)
    rank = mm(hit_b, before)
    sel = jnp.where(rank == (slot_row % CAP).astype(F32), hit_f, 0.0).astype(BF16)
    sel_v[...] = sel
    eye = jnp.where(
        lax.broadcasted_iota(jnp.int32, (S, S), 0) == lax.broadcasted_iota(jnp.int32, (S, S), 1), 1.0, 0.0
    ).astype(BF16)
    selt_v[0] = mm_nt(eye, sel)
    selt_v[1] = mm_nt(eye, hit_b)
    spread_e = jnp.where(
        lax.broadcasted_iota(jnp.int32, (L, EP), 0) // CAP == lax.broadcasted_iota(jnp.int32, (L, EP), 1), 1.0, 0.0
    ).astype(BF16)
    groups = grt_h.shape[0]
    spread_g = jnp.where(
        lax.broadcasted_iota(jnp.int32, (L, groups), 0) // (CAP * GS)
        == lax.broadcasted_iota(jnp.int32, (L, groups), 1),
        1.0,
        0.0,
    ).astype(BF16)
    for rd in range(NZ):
        cols = pl.ds(rows(0, rd), 128)
        rexp[rd, 0:L] = mm(spread_e, ert_v[:, cols]).astype(BF16)
        rexp[rd, L : 2 * L] = mm(spread_g, grt_v[:, cols]).astype(BF16)
    taps = par_v[6:10, :]
    bias = par_v[2:3, :]
    loads[k_conv].wait()
    conv_part = bias + sum(taps[j : j + 1, :] * conv_v[j].astype(F32) for j in range(3))

    loads[k_bw].wait()
    loads[k_gw].wait()

    def gather_and(buf, rsem, fsem, use, extra=None):
        prev = None
        for rd in near_first:
            if rd != 0:
                wait(buf.at[rd, 0], rsem.at[rd, 0])
                send(buf.at[rd, 0], buf.at[rd, 1], fsem.at[rd], rsem.at[rd, 1], partner)
                if extra is not None:
                    xb, xr, xf = extra
                    wait(xb.at[rd, 0], xr.at[rd, 0])
                    send(xb.at[rd, 0], xb.at[rd, 1], xf.at[rd], xr.at[rd, 1], partner)
            if prev is not None:
                wait(buf.at[prev, 1], rsem.at[prev, 1])
                if extra is not None:
                    wait(extra[0].at[prev, 1], extra[1].at[prev, 1])
                use(prev)
            prev = rd
        wait(buf.at[prev, 1], rsem.at[prev, 1])
        if extra is not None:
            wait(extra[0].at[prev, 1], extra[1].at[prev, 1])
        use(prev)

    sums = [jnp.zeros((S, 128), F32)] * 3

    def use_a(rd):
        x0 = tok_a[rd, 0].astype(F32)
        x1 = tok_a[rd, 1].astype(F32)
        sums[0] = sums[0] + x0 * x0 + x1 * x1
        g0 = gain_a[rd, 0][0:1, :]
        g1 = gain_a[rd, 1][0:1, :]
        xg = jnp.concatenate([(x0 * g0).astype(BF16), (x1 * g1).astype(BF16)], axis=1)
        i0 = pl.ds(rows(0, rd), 128)
        i1 = pl.ds(rows(1, rd), 128)
        sums[1] = sums[1] + mm(xg, jnp.concatenate([bw_v[i0, :], bw_v[i1, :]], axis=0))
        sums[2] = sums[2] + mm(xg, jnp.concatenate([gw_v[i0, :], gw_v[i1, :]], axis=0))

    gather_and(tok_a, r_a, f_a, use_a, (gain_a, r_g, f_g))
    rstd = lax.rsqrt(jnp.sum(sums[0], axis=1, keepdims=True) / WIDTH + EPS)
    branch = (sums[1] * rstd).astype(BF16)
    gating = (sums[2] * rstd).astype(BF16).astype(F32)
    branch_v[...] = branch

    conv_out = conv_part + taps[3:4, :] * branch.astype(F32)
    conv_low = conv_out.astype(BF16)
    loads[k_rw].wait()
    loads[k_iw].wait()
    loads[k_state].wait()
    recur_gate = sigmoid(mm(conv_low, rw_v[...]) + par_v[3:4, :])
    input_gate = sigmoid(mm(conv_low, iw_v[...]) + par_v[4:5, :])
    log_decay = 8.0 * recur_gate * log_sigmoid(par_v[5:6, :])
    new_state = jnp.exp(log_decay) * state_v[...] + jnp.sqrt(expm1_neg(2.0 * log_decay)) * (
        input_gate * conv_out
    )
    nstate_v[...] = new_state
    hid_b[0, 0] = (new_state * gelu(gating)).astype(BF16)

    for d in far_first:
        rd = back_rel(d)
        send(hid_b.at[0, 0], hid_b.at[rd, 0], s_b.at[d], r_b.at[rd, 0], zdev(d))
    send(hid_b.at[0, 0], hid_b.at[0, 1], f_b.at[0], r_b.at[0, 1], partner)
    out_state = pltpu.make_async_copy(nstate_v, nstate_h, sem_o.at[0])
    out_state.start()
    out_conv = pltpu.make_async_copy(conv_v.at[1:3], nconv_h.at[0:2], sem_o.at[1])
    out_conv.start()
    out_branch = pltpu.make_async_copy(branch_v, nconv_h.at[2], sem_o.at[2])
    out_branch.start()
    loads[k_w[0]].wait()
    send(wdn.at[0, 0], wdn.at[0, 1], f_w.at[0], r_w.at[0, 1], partner)
    for rd in near_first[1:]:
        wait(wdn.at[rd, 0], r_w.at[rd, 0])
        send(wdn.at[rd, 0], wdn.at[rd, 1], f_w.at[rd], r_w.at[rd, 1], partner)
    loads[k_ow].wait()
    proj = [jnp.zeros((S, 128), F32)]

    def use_b(rd):
        h = jnp.concatenate([hid_b[rd, 0], hid_b[rd, 1]], axis=1)
        w = jnp.concatenate([ow_v[pl.ds(rows(0, rd), 128), :], ow_v[pl.ds(rows(1, rd), 128), :]], axis=0)
        proj[0] = proj[0] + mm(h, w)

    gather_and(hid_b, r_b, f_b, use_b)
    resid = (tok_a[0, 0].astype(F32) + proj[0]).astype(BF16)
    res_c[0] = resid

    for d in far_first:
        rd = back_rel(d)
        send(res_c.at[0], res_c.at[rd], s_c.at[d], r_c.at[rd], zdev(d))
    ss_row = jnp.zeros((S, 128), F32)
    for rd in near_first:
        if rd != 0:
            wait(res_c.at[rd], r_c.at[rd])
        x = res_c[rd]
        rows_out = mm(sel_v[...], x).astype(BF16)
        ysel[rd] = rows_out.reshape(EP, CAP, 128)

        def dispatch(i, carry):
            e = (me + i) % EP
            send(ysel.at[rd, e], xbuf.at[rd, me], s_d.at[rd], r_d.at[rd], (e, tp))
            return carry

        lax.fori_loop(1, EP, dispatch, 0)
        xbuf[rd, me] = ysel[rd, me]
        xf = x.astype(F32)
        ss_row = ss_row + xf * xf
        xg = (xf * gain_a[rd, 0][1:2, :]).astype(BF16)
        part = mm_nt(xg, rexp[rd])
        if rd == 0:
            lg_own[...] = part
        else:
            lg_own[...] += part
    ss_own[...] = ss_row
    send(lg_own, lg_in, s_l.at[0], r_l.at[0], partner)
    send(ss_own, ss_in, s_l.at[1], r_l.at[1], partner)

    for k in k_x:
        loads[k].wait()
    for rd in range(NZ):
        wait(wcat.at[rd, 1], r_x.at[rd, 0])
        wait(wcat.at[rd, 3], r_x.at[rd, 1])
    for n, rd in enumerate(near_first):
        wait(xbuf.at[rd, 0 : EP - 1], r_d.at[rd])
        xf = xbuf[rd].reshape(L, 128).astype(F32)
        xg = (xf * gain_a[rd, 0][1:2, :]).astype(BF16)
        part = mm_nt(xg, wcat[rd].reshape(256, 128))
        if n == 0:
            ssx_v[...] = xf * xf
            acc_v[...] = part
        else:
            ssx_v[...] += xf * xf
            acc_v[...] += part
    theirs = pl.ds(pl.multiple_of(other * HALF, HALF), HALF)
    ours = pl.ds(pl.multiple_of(c * HALF, HALF), HALF)
    send(acc_v.at[theirs], pacc_v, s_p.at[0], r_p.at[0], partner)
    send(ssx_v.at[theirs], pss_v, s_p.at[1], r_p.at[1], partner)

    wait(lg_in, r_l.at[0])
    wait(ss_in, r_l.at[1])
    ss_tot = jnp.sum(ss_own[...] + ss_in[...], axis=1, keepdims=True)
    rstd2 = lax.rsqrt(ss_tot / WIDTH + EPS)
    logits = (lg_own[...] + lg_in[...]) * rstd2
    e_exp = jnp.exp(logits[:, 0:L])
    g_exp = jnp.exp(logits[:, L : 2 * L])
    e_den = jnp.sum(e_exp * selt_v[1], axis=1, keepdims=True) * (1.0 / CAP)
    g_den = jnp.sum(g_exp, axis=1, keepdims=True) * (1.0 / (CAP * GS))
    combine = selt_v[0] * (g_exp / g_den) * (e_exp / e_den)
    comb_hi = combine.astype(BF16)
    comb_lo = (combine - comb_hi.astype(F32)).astype(BF16)

    wait(pacc_v, r_p.at[0])
    wait(pss_v, r_p.at[1])
    ss_slot = jnp.sum(ssx_v[ours, :] + pss_v[...], axis=1, keepdims=True)
    rstd_slot = lax.rsqrt(ss_slot / WIDTH + EPS)
    mine = acc_v[ours, :]
    theirs_in = pacc_v[...]
    def reorder(v):
        return jnp.concatenate([v[:, 64:128], v[:, 0:64], v[:, 192:256], v[:, 128:192]], axis=1)

    gu = (mine + reorder(theirs_in)) * rstd_slot
    gate = gu[:, 0:128]
    hid_e[0] = (gate * sigmoid(gate) * gu[:, 128:256]).astype(BF16)

    for d in far_first:
        rd = back_rel(d)
        send(hid_e.at[0], hid_e.at[rd], s_e.at[d], r_e.at[rd], zdev(d))
    for rd in range(NZ):
        wait(wdn.at[rd, 1], r_w.at[rd, 1])
    out = [None]
    for rd in near_first:
        if rd != 0:
            wait(hid_e.at[rd], r_e.at[rd])
        part = mm(hid_e[rd], wdn[rd].reshape(128, 256))
        out[0] = part if out[0] is None else out[0] + part
    y = out[0].astype(BF16)
    y_v[0] = y[:, 0:128].reshape(HS, CAP, 128)
    y_v[1] = y[:, 128:256].reshape(HS, CAP, 128)

    def give_back(i, carry):
        s = c * HS + i

        @pl.when(s != me)
        def _():
            send(y_v.at[c, i], back_v.at[me], s_f.at[i, 0], r_f.at[0], (s, tp))

        send(y_v.at[other, i], back_v.at[me], s_f.at[i, 1], r_f.at[0], (s, 2 * z + other))
        return carry

    lax.fori_loop(0, HS, give_back, 0)
    own_half = me // HS == c

    @pl.when(own_half)
    def _():
        back_v[me] = y_v[c, me - c * HS]
        wait(back_v.at[0 : EP - 1], r_f.at[0])

    @pl.when(jnp.logical_not(own_half))
    def _():
        wait(back_v, r_f.at[0])

    back = back_v[...].reshape(L, 128)
    moe = mm(comb_hi, back) + mm(comb_lo, back)
    mixed_v[...] = (res_c[0].astype(F32) + moe).astype(BF16)
    out_mixed = pltpu.make_async_copy(mixed_v, mixed_h, sem_o.at[3])
    out_mixed.start()

    for d in range(1, NZ):
        wait(gain_a.at[0, 0], s_g.at[d])
        wait(tok_a.at[0, 0], s_a.at[d])
        wait(wdn.at[0, 0], s_w.at[d])
        wait(hid_b.at[0, 0], s_b.at[d])
        wait(res_c.at[0], s_c.at[d])
        wait(hid_e.at[0], s_e.at[d])
    for rd in range(NZ):
        wait(gain_a.at[0, 0], f_g.at[rd])
        wait(tok_a.at[0, 0], f_a.at[rd])
        wait(wdn.at[0, 0], f_w.at[rd])
        wait(hid_b.at[0, 0], f_b.at[rd])
        wait(wcat.at[0, 0], s_x.at[rd, 0])
        wait(wcat.at[0, 0], s_x.at[rd, 1])
        wait(ysel.at[rd, 0 : EP - 1], s_d.at[rd])
    wait(lg_own, s_l.at[0])
    wait(ss_own, s_l.at[1])
    wait(pacc_v, s_p.at[0])
    wait(pss_v, s_p.at[1])

    def left(i, carry):
        @pl.when(c * HS + i != me)
        def _():
            wait(y_v.at[0, 0], s_f.at[i, 0])

        wait(y_v.at[0, 0], s_f.at[i, 1])
        return carry

    lax.fori_loop(0, HS, left, 0)
    out_state.wait()
    out_conv.wait()
    out_branch.wait()
    out_mixed.wait()


def on_device(
    tokens, conv_state, recur_state, norm1_gain, branch_weight, gating_weight, conv_taps, conv_bias,
    recur_weight, recur_bias, input_weight, input_bias, decay_logit, out_weight, norm2_gain,
    group_router, expert_router, routes, gate_experts, up_experts, down_experts,
):
    EP = lax.axis_size("ep")
    TPN = lax.axis_size("tp")
    NZ = TPN // 2
    S = tokens.shape[0]
    CAP = 2 * routes.shape[1] * S // EP
    GS = expert_router.shape[1] // group_router.shape[1]
    L = EP * CAP
    par = jnp.concatenate(
        [
            jnp.stack(
                [
                    norm1_gain.astype(F32),
                    norm2_gain.astype(F32),
                    conv_bias.astype(F32),
                    recur_bias,
                    input_bias,
                    decay_logit,
                ]
            ),
            conv_taps.astype(F32),
            jnp.zeros((6, 128), F32),
        ],
        axis=0,
    )
    args = (
        tokens,
        jnp.transpose(conv_state, (1, 0, 2)),
        recur_state,
        par,
        branch_weight,
        gating_weight,
        recur_weight[0],
        input_weight[0],
        out_weight,
        group_router.T,
        expert_router.T,
        routes.T,
        gate_experts[0].T,
        up_experts[0].T,
        down_experts[0],
    )
    D = TPN * 128
    V = pltpu.VMEM
    dma = pltpu.SemaphoreType.DMA
    scratch = [
        V((NZ, 2, S, 128), BF16),
        V((NZ, 2, 2, 128), F32),
        V((3, S, 128), BF16),
        V((S, 128), F32),
        V((16, 128), F32),
        V((D, 128), BF16),
        V((D, 128), BF16),
        V((128, 128), BF16),
        V((128, 128), BF16),
        V((D, 128), BF16),
        V(args[9].shape, BF16),
        V(args[10].shape, BF16),
        V((2, S), jnp.int32),
        V((NZ, 4, 64, 128), BF16),
        V((NZ, 2, 64, 256), BF16),
        V((NZ, 2, S, 128), BF16),
        V((NZ, S, 128), BF16),
        V((NZ, EP, CAP, 128), BF16),
        V((NZ, EP, CAP, 128), BF16),
        V((NZ, 2 * L, 128), BF16),
        V((S, 2 * L), F32),
        V((S, 2 * L), F32),
        V((S, 128), F32),
        V((S, 128), F32),
        V((L, 256), F32),
        V((L // 2, 256), F32),
        V((L, 128), F32),
        V((L // 2, 128), F32),
        V((NZ, L // 2, 128), BF16),
        V((2, EP // 2, CAP, 128), BF16),
        V((EP, CAP, 128), BF16),
        V((S, 128), BF16),
        V((S, 128), F32),
        V((S, 128), BF16),
        V((L, S), BF16),
        V((2, S, L), F32),
        dma((13 + 2 * NZ,)),
        dma((NZ,)), dma((NZ, 2)), dma((NZ,)),
        dma((NZ,)), dma((NZ, 2)), dma((NZ,)),
        dma((NZ,)), dma((NZ, 2)), dma((NZ,)),
        dma((NZ,)), dma((NZ, 2)), dma((NZ,)),
        dma((NZ, 2)), dma((NZ, 2)),
        dma((NZ,)), dma((NZ,)),
        dma((NZ,)), dma((NZ,)),
        dma((2,)), dma((2,)),
        dma((2,)), dma((2,)),
        dma((NZ,)), dma((NZ,)),
        dma((EP // 2, 2)), dma((1,)),
        dma((4,)),
    ]
    anyspace = pl.BlockSpec(memory_space=pl.ANY)
    mixed, new_state, new_conv = pl.pallas_call(
        functools.partial(kernel, EP, NZ, S, CAP, GS),
        out_shape=(
            jax.ShapeDtypeStruct((S, 128), BF16),
            jax.ShapeDtypeStruct((S, 128), F32),
            jax.ShapeDtypeStruct((3, S, 128), BF16),
        ),
        in_specs=[anyspace] * len(args),
        out_specs=[anyspace] * 3,
        scratch_shapes=scratch,
        compiler_params=pltpu.CompilerParams(
            collective_id=0, has_side_effects=True, vmem_limit_bytes=40 * 1024 * 1024
        ),
        name="layer",
    )(*args)
    return mixed, new_state, jnp.transpose(new_conv, (1, 0, 2))


def solution(mesh):
    return jax.shard_map(
        on_device,
        mesh=mesh,
        in_specs=(
            P("ep", "tp"),
            P("ep", None, "tp"),
            P("ep", "tp"),
            P("tp"),
            P(None, "tp"),
            P(None, "tp"),
            P(None, "tp"),
            P("tp"),
            P("tp", None, None),
            P("tp"),
            P("tp", None, None),
            P("tp"),
            P("tp"),
            P(None, "tp"),
            P("tp"),
            P(),
            P(),
            P("ep", None),
            P("ep", None, "tp"),
            P("ep", None, "tp"),
            P("ep", "tp", None),
        ),
        out_specs=(P("ep", "tp"), P("ep", "tp"), P("ep", None, "tp")),
        check_vma=False,
    )
```

time: 152 us -> 77.6 us (0.51)
  blocking collectives: 70.5 us -> 0 us
  Pallas kernels: 0 us -> 60.9 us
  waiting for transfers between devices: 39.3 us -> 0 us
  starting transfers between devices: 24.8 us -> 0 us
  local copies, waits for them, and re-layouts: 4.15 us -> 13.9 us
  matrix products: 5.39 us -> 0 us
  other arithmetic: 6.55 us -> 1.35 us
    all_to_all x3 -> x0, blocking collectives: 70.5 us -> none  [the longest x1 31.6 us: sent_and_summed(): blocks = lax.all_to_all(split_up(array, dim, count), axis, 0, 0, tiled=True)]
    pallas_call x0 -> x1, Pallas kernels: none -> 60.9 us  [on_device(): pl.pallas_call(functools.partial(kernel, EP, NZ, S, CAP, GS), out_shape=(...]
    all_to_all x5 -> x0, waiting for transfers between devices: 39.3 us -> none  [the longest x4 33.4 us: from_everyone(): lax.all_to_all(jnp.broadcast_to(array[None], (count, *array.shape)), axis...]
    all_to_all x5 -> x0, starting transfers between devices: 24.8 us -> none  [the longest x4 21.3 us: from_everyone(): lax.all_to_all(jnp.broadcast_to(array[None], (count, *array.shape)), axis...]
    unnamed x35 -> x31, local copies, waits for them, and re-layouts: 0.78 us -> 12.4 us
    dot_general x11 -> x0, matrix products: 5.39 us -> none  [the longest x1 1.26 us: on_device(): jnp.einsum('sacf,afd->sacd', hidden, down_experts, preferred_element_type...]
    convert_element_type x7 -> x0, other arithmetic: 2.95 us -> none  [the longest x1 0.8 us: on_device(): (tok_float * rstd_one * norm1_gain.astype(jnp.float32)).astype(jnp.bfloat16)]
    broadcast_in_dim x5 -> x1, local copies, waits for them, and re-layouts: 2.76 us -> 0.01 us  [on_device(): jnp.zeros((6, 128), F32)]
  transfers between devices with their start and end apart: 5 -> 0, of which waited for: 5 -> 0; matrix products, arithmetic and copies ran while one was open for 3% -> 0% of each run, Pallas kernels for 0% -> 0%
where the time goes in v1:
time: 77.6 us; the launch traced here: 76.8 us
  Pallas kernels  60.9 us (78%)
  local copies, waits for them, and re-layouts  13.9 us (18%)
  other arithmetic  1.35 us (2%)
    pallas_call x1, Pallas kernels, on_device(): pl.pallas_call(functools.partial(kernel, EP, NZ, S, CAP, GS), out_shape=(...  60.9 us
    unnamed x31, local copies, waits for them, and re-layouts  12.4 us

profile of v1, /device:TPU:1, one launch (start us, length us, event | category | flops | bytes accessed | tf_op | source)
XLA Modules:
  0.0 76.8 jit_solution(2112481372557107980)
XLA Ops:
  0.6 0.0 copy-start.7
  0.6 0.7 bitcast_convert_fusion.2
  1.3 0.7 bitcast_convert_fusion
  2.0 0.0 copy-start.13
  2.0 1.5 %concatenate.3.par_h = f32[16,128]{1,0:T(8,128)S(1)} concatenate(f32[1,128]{1,0:T(1,128)S(1)} %bitcast_convert_fusion.2, f32[1,128]{1,0:T(1,128)S(1)} %get-tuple-element.10, f32[1,128]{1,0:T(1,128)S(1)} %get-tuple-element.9, f32[1,128]{1,0:T(1,128)} %bitcast.36, f32[1,128]{1,0:T(1,128)} %bitcast.37, f32[1,128]{1,0:T(1,128)} %bitcast.38, bf16[4,128]{1,0:T(4,128)(2,1)} %param.27, ...), dimensions={0} | concatenate | bytes 15360 | tf_op jit(solution)/shard_map/concatenate | solution.py:452
  3.5 0.0 copy-done.7
  3.5 0.0 copy-done.13
  3.5 0.0 copy-start
  3.5 1.0 %copy-done = bf16[2048,128]{1,0:T(8,128)(2,1)S(1)} copy-done((bf16[2048,128]{1,0:T(8,128)(2,1)S(1)}, bf16[2048,128]{1,0:T(8,128)(2,1)}, u32[]{:S(2)}) %copy-start) | copy-done | bytes 524312
  4.5 0.0 copy-start.1
  4.5 1.0 %copy-done.1 = bf16[2048,128]{1,0:T(8,128)(2,1)S(1)} copy-done((bf16[2048,128]{1,0:T(8,128)(2,1)S(1)}, bf16[2048,128]{1,0:T(8,128)(2,1)}, u32[]{:S(2)}) %copy-start.1) | copy-done | bytes 524312
  5.6 0.0 copy-start.2
  5.6 1.0 %copy-done.2 = bf16[2048,128]{1,0:T(8,128)(2,1)S(1)} copy-done((bf16[2048,128]{1,0:T(8,128)(2,1)S(1)}, bf16[2048,128]{1,0:T(8,128)(2,1)}, u32[]{:S(2)}) %copy-start.2) | copy-done | bytes 524312
  6.6 0.0 copy-start.3
  6.6 0.9 %copy-done.3 = bf16[1,2048,64]{1,2,0:T(8,128)(2,1)S(1)} copy-done((bf16[1,2048,64]{1,2,0:T(8,128)(2,1)S(1)}, bf16[1,2048,64]{1,2,0:T(8,128)(2,1)}, u32[]{:S(2)}) %copy-start.3) | copy-done | bytes 262168
  7.6 0.0 copy-start.4
  7.6 0.9 %copy-done.4 = bf16[1,2048,64]{1,2,0:T(8,128)(2,1)S(1)} copy-done((bf16[1,2048,64]{1,2,0:T(8,128)(2,1)S(1)}, bf16[1,2048,64]{1,2,0:T(8,128)(2,1)}, u32[]{:S(2)}) %copy-start.4) | copy-done | bytes 262168
  8.5 0.0 copy-start.5
  8.5 0.9 %copy-done.5 = bf16[1,64,2048]{2,1,0:T(8,128)(2,1)S(1)} copy-done((bf16[1,64,2048]{2,1,0:T(8,128)(2,1)S(1)}, bf16[1,64,2048]{2,1,0:T(8,128)(2,1)}, u32[]{:S(2)}) %copy-start.5) | copy-done | bytes 262168
  9.5 0.0 copy-start.6
  9.5 0.8 %copy-done.6 = bf16[2048,16]{0,1:T(8,128)(2,1)S(1)} copy-done((bf16[2048,16]{0,1:T(8,128)(2,1)S(1)}, bf16[2048,16]{0,1:T(8,128)(2,1)}, u32[]{:S(2)}) %copy-start.6) | copy-done | bytes 65560
  10.3 0.0 copy-start.8
  10.3 0.8 copy-done.8
  11.1 0.0 copy-start.9
  11.1 0.8 copy-done.9
  11.8 0.0 copy-start.10
  11.8 0.8 copy-done.10
  12.6 0.0 copy-start.11
  12.6 0.7 copy-done.11
  13.3 0.0 copy-start.12
  13.3 0.7 copy-done.12
  14.0 60.9 %layer.1 = (bf16[64,128]{1,0:T(8,128)(2,1)S(1)}, f32[64,128]{1,0:T(8,128)S(1)}, bf16[3,64,128]{2,1,0:T(8,128)(2,1)S(1)}) custom-call(bf16[64,128]{1,0:T(8,128)(2,1)S(1)} %copy-done.11, bf16[3,64,128]{2,1,0:T(8,128)(2,1)S(1)} %bitcast.31, f32[64,128]{1,0:T(8,128)S(1)} %copy-done.8, f32[16,128]{1,0:T(8,128)S(1)} %concatenate.3.par_h, ...), custom_call_target="tpu_custom_call" | custom-call | tf_op jit(solution)/shard_map/layer/pallas_call | solution.py:541
  74.9 0.6 copy.27
  75.5 0.6 copy.28
  76.2 0.6 copy.29
  (1 shorter events, 0.0 us)
Async XLA Ops:
  0.6 2.9 %copy-start.7 = (bf16[64,3,128]{2,0,1:T(8,128)(2,1)S(1)}, bf16[64,3,128]{2,0,1:T(8,128)(2,1)}, u32[]{:S(2)}) copy-start(bf16[64,3,128]{2,0,1:T(8,128)(2,1)} %param.22) | copy-start | bytes 147460
  2.0 1.5 %copy-start.13 = (s32[64,2]{0,1:T(2,128)S(1)}, s32[64,2]{0,1:T(2,128)}, u32[]{:S(2)}) copy-start(s32[64,2]{0,1:T(2,128)} %param.38) | copy-start | bytes 1540
  3.5 1.0 %copy-start = (bf16[2048,128]{1,0:T(8,128)(2,1)S(1)}, bf16[2048,128]{1,0:T(8,128)(2,1)}, u32[]{:S(2)}) copy-start(bf16[2048,128]{1,0:T(8,128)(2,1)} %bw_h.1) | copy-start | bytes 1572868
  4.5 1.0 %copy-start.1 = (bf16[2048,128]{1,0:T(8,128)(2,1)S(1)}, bf16[2048,128]{1,0:T(8,128)(2,1)}, u32[]{:S(2)}) copy-start(bf16[2048,128]{1,0:T(8,128)(2,1)} %gw_h.1) | copy-start | bytes 1572868
  5.6 1.0 %copy-start.2 = (bf16[2048,128]{1,0:T(8,128)(2,1)S(1)}, bf16[2048,128]{1,0:T(8,128)(2,1)}, u32[]{:S(2)}) copy-start(bf16[2048,128]{1,0:T(8,128)(2,1)} %ow_h.1) | copy-start | bytes 1572868
  6.6 0.9 %copy-start.3 = (bf16[1,2048,64]{1,2,0:T(8,128)(2,1)S(1)}, bf16[1,2048,64]{1,2,0:T(8,128)(2,1)}, u32[]{:S(2)}) copy-start(bf16[1,2048,64]{1,2,0:T(8,128)(2,1)} %param.39) | copy-start | bytes 786436
  7.6 0.9 %copy-start.4 = (bf16[1,2048,64]{1,2,0:T(8,128)(2,1)S(1)}, bf16[1,2048,64]{1,2,0:T(8,128)(2,1)}, u32[]{:S(2)}) copy-start(bf16[1,2048,64]{1,2,0:T(8,128)(2,1)} %param.40) | copy-start | bytes 786436
  8.5 0.9 %copy-start.5 = (bf16[1,64,2048]{2,1,0:T(8,128)(2,1)S(1)}, bf16[1,64,2048]{2,1,0:T(8,128)(2,1)}, u32[]{:S(2)}) copy-start(bf16[1,64,2048]{2,1,0:T(8,128)(2,1)} %param.41) | copy-start | bytes 786436
  9.5 0.8 %copy-start.6 = (bf16[2048,16]{0,1:T(8,128)(2,1)S(1)}, bf16[2048,16]{0,1:T(8,128)(2,1)}, u32[]{:S(2)}) copy-start(bf16[2048,16]{0,1:T(8,128)(2,1)} %param.37) | copy-start | bytes 196612
  10.3 0.8 copy-start.8
  11.1 0.8 copy-start.9
  11.8 0.8 copy-start.10
  12.6 0.7 copy-start.11
  13.3 0.7 copy-start.12

commit v2 on v1

--- a/solution.py
+++ b/solution.py
@@ -47,9 +47,9 @@
 
 def kernel(
     EP, NZ, S, CAP, GS,
-    tok_h, conv_h, state_h, par_h, bw_h, gw_h, rw_h, iw_h, ow_h, grt_h, ert_h, rt_h, gt_h, ut_h, dn_h,
+    tok_h, conv_h, state_h, n1_h, n2_h, cb_h, rb_h, ib_h, dl_h, taps_h, bw_h, gw_h, rw_h, iw_h, ow_h, grt_h, ert_h, rt_h, gt_h, ut_h, dn_h,
     mixed_h, nstate_h, nconv_h,
-    tok_a, gain_a, conv_v, state_v, par_v, bw_v, gw_v, rw_v, iw_v, ow_v, grt_v, ert_v, rt_v, wcat, wdn,
+    tok_a, gain_a, conv_v, state_v, n1_v, n2_v, cb_v, rb_v, ib_v, dl_v, taps_v, bw_v, gw_v, rw_v, iw_v, ow_v, grt_v, ert_v, rt_v, wcat, wdn,
     hid_b, res_c, ysel, xbuf, rexp, lg_own, lg_in, ss_own, ss_in, acc_v, pacc_v, ssx_v, pss_v,
     hid_e, y_v, back_v, mixed_v, nstate_v, branch_v, sel_v, selt_v,
     sem_ld, s_a, r_a, f_a, s_g, r_g, f_g, s_b, r_b, f_b, s_w, r_w, f_w, s_x, r_x,
@@ -82,6 +82,9 @@
     far_first = sorted(range(1, NZ), key=lambda d: (-min(d, NZ - d), d))
     near_first = [0] + sorted(range(1, NZ), key=lambda d: (min(d, NZ - d), d))
 
+    def row(ref):
+        return ref[...].astype(F32).reshape(1, 128)
+
     def wait(ref, sem):
         pltpu.make_async_copy(ref, ref, sem).wait()
 
@@ -100,7 +103,8 @@
         return k
 
     k_tok = load(tok_h, tok_a.at[0, 0])
-    k_par = load(par_h, par_v)
+    k_n1 = load(n1_h, n1_v)
+    k_n2 = load(n2_h, n2_v)
     k_rt = load(rt_h, rt_v)
 
     bar = pltpu.get_barrier_semaphore()
@@ -120,6 +124,7 @@
 
     lax.fori_loop(1, EP, bar_ep, 0)
 
+    k_small = [load(a, b) for a, b in ((cb_h, cb_v), (rb_h, rb_v), (ib_h, ib_v), (dl_h, dl_v), (taps_h, taps_v))]
     k_conv = load(conv_h, conv_v)
     k_state = load(state_h, state_v)
     k_bw = load(bw_h, bw_v)
@@ -137,8 +142,9 @@
         k_x.append(load(ut_h.at[:, cols], wcat.at[rd, 2]))
 
     loads[k_tok].wait()
-    loads[k_par].wait()
-    gain_a[0, 0] = par_v[0:2, :]
+    loads[k_n1].wait()
+    loads[k_n2].wait()
+    gain_a[0, 0] = jnp.concatenate([row(n1_v), row(n2_v)], axis=0)
 
     pl.semaphore_wait(bar, (NZ - 1) + 1 + 2 * (EP - 1))
 
@@ -192,8 +198,10 @@
         cols = pl.ds(rows(0, rd), 128)
         rexp[rd, 0:L] = mm(spread_e, ert_v[:, cols]).astype(BF16)
         rexp[rd, L : 2 * L] = mm(spread_g, grt_v[:, cols]).astype(BF16)
-    taps = par_v[6:10, :]
-    bias = par_v[2:3, :]
+    for k in k_small:
+        loads[k].wait()
+    taps = taps_v[...].astype(F32)
+    bias = row(cb_v)
     loads[k_conv].wait()
     conv_part = bias + sum(taps[j : j + 1, :] * conv_v[j].astype(F32) for j in range(3))
 
@@ -246,9 +254,9 @@
     loads[k_rw].wait()
     loads[k_iw].wait()
     loads[k_state].wait()
-    recur_gate = sigmoid(mm(conv_low, rw_v[...]) + par_v[3:4, :])
-    input_gate = sigmoid(mm(conv_low, iw_v[...]) + par_v[4:5, :])
-    log_decay = 8.0 * recur_gate * log_sigmoid(par_v[5:6, :])
+    recur_gate = sigmoid(mm(conv_low, rw_v[...]) + row(rb_v))
+    input_gate = sigmoid(mm(conv_low, iw_v[...]) + row(ib_v))
+    log_decay = 8.0 * recur_gate * log_sigmoid(row(dl_v))
     new_state = jnp.exp(log_decay) * state_v[...] + jnp.sqrt(expm1_neg(2.0 * log_decay)) * (
         input_gate * conv_out
     )
@@ -449,28 +457,17 @@
     CAP = 2 * routes.shape[1] * S // EP
     GS = expert_router.shape[1] // group_router.shape[1]
     L = EP * CAP
-    par = jnp.concatenate(
-        [
-            jnp.stack(
-                [
-                    norm1_gain.astype(F32),
-                    norm2_gain.astype(F32),
-                    conv_bias.astype(F32),
-                    recur_bias,
-                    input_bias,
-                    decay_logit,
-                ]
-            ),
-            conv_taps.astype(F32),
-            jnp.zeros((6, 128), F32),
-        ],
-        axis=0,
-    )
     args = (
         tokens,
         jnp.transpose(conv_state, (1, 0, 2)),
         recur_state,
-        par,
+        norm1_gain,
+        norm2_gain,
+        conv_bias,
+        recur_bias,
+        input_bias,
+        decay_logit,
+        conv_taps,
         branch_weight,
         gating_weight,
         recur_weight[0],
@@ -491,14 +488,16 @@
         V((NZ, 2, 2, 128), F32),
         V((3, S, 128), BF16),
         V((S, 128), F32),
-        V((16, 128), F32),
+        V((128,), BF16), V((128,), BF16), V((128,), BF16),
+        V((128,), F32), V((128,), F32), V((128,), F32),
+        V((4, 128), BF16),
         V((D, 128), BF16),
         V((D, 128), BF16),
         V((128, 128), BF16),
         V((128, 128), BF16),
         V((D, 128), BF16),
-        V(args[9].shape, BF16),
-        V(args[10].shape, BF16),
+        V(group_router.T.shape, BF16),
+        V(expert_router.T.shape, BF16),
         V((2, S), jnp.int32),
         V((NZ, 4, 64, 128), BF16),
         V((NZ, 2, 64, 256), BF16),
@@ -523,7 +522,7 @@
         V((S, 128), BF16),
         V((L, S), BF16),
         V((2, S, L), F32),
-        dma((13 + 2 * NZ,)),
+        dma((20 + 2 * NZ,)),
         dma((NZ,)), dma((NZ, 2)), dma((NZ,)),
         dma((NZ,)), dma((NZ, 2)), dma((NZ,)),
         dma((NZ,)), dma((NZ, 2)), dma((NZ,)),
@@ -549,7 +548,7 @@
         out_specs=[anyspace] * 3,
         scratch_shapes=scratch,
         compiler_params=pltpu.CompilerParams(
-            collective_id=0, has_side_effects=True, vmem_limit_bytes=40 * 1024 * 1024
+            collective_id=0, has_side_effects=True, vmem_limit_bytes=67_000_000
         ),
         name="layer",
     )(*args)

time: 77.6 us -> 64.9 us (0.84)
  local copies, waits for them, and re-layouts: 13.9 us -> 2.59 us
  other arithmetic: 1.35 us -> 0 us
    unnamed x31 -> x7, local copies, waits for them, and re-layouts: 12.4 us -> 2.59 us
    concatenate x1 -> x0, local copies, waits for them, and re-layouts: 1.5 us -> none  [on_device(): jnp.concatenate([jnp.stack([norm1_gain.astype(F32), norm2_gain.astype(F32...]
    another operation x2 -> x0, other arithmetic: 1.35 us -> none  [on_device(): jnp.stack([norm1_gain.astype(F32), norm2_gain.astype(F32), conv_bias.asty...]
where the time goes in v2:
time: 64.9 us; the launch traced here: 64.7 us
  Pallas kernels  61.5 us (95%)
  local copies, waits for them, and re-layouts  2.59 us (4%)
  between operations  0.67 us (1%)
    pallas_call x1, Pallas kernels, on_device(): pl.pallas_call(functools.partial(kernel, EP, NZ, S, CAP, GS), out_shape=(...  61.5 us
    unnamed x7, local copies, waits for them, and re-layouts  2.59 us

profile of v2, /device:TPU:1, one launch (start us, length us, event | category | flops | bytes accessed | tf_op | source)
XLA Modules:
  0.0 64.7 jit_solution(5377306063749743777)
XLA Ops:
  0.6 61.5 %layer.1 = (bf16[64,128]{1,0:T(8,128)(2,1)}, f32[64,128]{1,0:T(8,128)}, bf16[3,64,128]{2,1,0:T(8,128)(2,1)}) custom-call(bf16[64,128]{1,0:T(8,128)(2,1)} %tok_h.1, bf16[3,64,128]{2,1,0:T(8,128)(2,1)} %bitcast.19, f32[64,128]{1,0:T(8,128)} %state_h.1, bf16[128]{0:T(256)(128)(2,1)} %n1_h.1, bf16[128]{0:T(256)(128)(2,1)} %n2_h.1, bf16[128]{0:T(256)(128)(2,1)} %cb_h.1, ...), custom_call_target="tpu_custom_call" | custom-call | tf_op jit(solution)/shard_map/layer/pallas_call | solution.py:540
  62.1 0.0 copy-start.1
  62.1 0.0 copy-start
  62.1 1.3 %copy.27 = bf16[64,128]{1,0:T(8,128)(2,1)} copy(bf16[64,128]{1,0:T(8,128)(2,1)} %get-tuple-element.12) | data formatting | bytes 32768
  63.5 0.0 copy-done.1
  63.5 0.6 copy.28
  64.1 0.0 copy-done
  64.1 0.6 copy.29
Async XLA Ops:
  62.1 1.4 %copy-start.1 = (f32[64,128]{1,0:T(8,128)S(1)}, f32[64,128]{1,0:T(8,128)}, u32[]{:S(2)}) copy-start(f32[64,128]{1,0:T(8,128)} %get-tuple-element.13) | copy-start | bytes 98308
  62.1 2.0 %copy-start = (bf16[3,64,128]{2,1,0:T(8,128)(2,1)S(1)}, bf16[3,64,128]{2,1,0:T(8,128)(2,1)}, u32[]{:S(2)}) copy-start(bf16[3,64,128]{2,1,0:T(8,128)(2,1)} %get-tuple-element.8) | copy-start | bytes 147460

commit v3 on v2

v3 whole, which is shorter than its diff:
```python
import functools

import jax
import jax.numpy as jnp
from jax import lax
from jax.experimental import pallas as pl
from jax.experimental.pallas import tpu as pltpu
from jax.sharding import PartitionSpec as P

EPS = 1e-06
NEAR = 2
F32 = jnp.float32
BF16 = jnp.bfloat16
MESH = pl.DeviceIdType.MESH
NT = (((1,), (1,)), ((), ()))


def mm(a, b):
    return jnp.dot(a, b, preferred_element_type=F32)


def mm_nt(a, b):
    return lax.dot_general(a, b, NT, preferred_element_type=F32)


def expm1_neg(x):
    series = x * (1.0 + x * (0.5 + x * (1.0 / 6 + x * (1.0 / 24 + x * (1.0 / 120 + x / 720)))))
    return jnp.where(x > -0.2, -series, 1.0 - jnp.exp(x))


def log_sigmoid(x):
    u = jnp.exp(-jnp.abs(x))
    w = u / (2.0 + u)
    w2 = w * w
    poly = 1.0 / 15
    for k in (13, 11, 9, 7, 5, 3, 1):
        poly = poly * w2 + 1.0 / k
    return jnp.minimum(x, 0.0) - 2.0 * w * poly


def gelu(x):
    return 0.5 * x * (1.0 + jnp.tanh(0.7978845608028654 * (x + 0.044715 * x * x * x)))


def sigmoid(x):
    return 1.0 / (1.0 + jnp.exp(-x))


def kernel(
    EP, NZ, S, CAP, GS,
    tok_h, conv_h, state_h, n1_h, n2_h, cb_h, rb_h, ib_h, dl_h, taps_h, bw_h, gw_h, rw_h, iw_h, ow_h,
    grt_h, ert_h, rt_h, gt_h, ut_h, dn_h,
    mixed_h, nstate_h, nconv_h,
    tok_v, tok_a, gain_a, conv_v, conv_p, state_p, n1_v, n2_v, cb_v, rb_v, ib_v, dl_v, taps_v, par_v,
    bw_p, gw_p, rw_p, iw_p, ow_p, grt_v, ert_v, rt_v, wcat, wdn,
    hid_b, res_c, res_x, ysel, yfar, xbuf, xfar, rexp, lg_own, lg_in, ss_own, ss_in, acc_v, ssx_v,
    hid_e, y_v, back_v, mixed_v, nstate_v, ns_x, branch_v, br_x, sel_v, selt_v,
    sem_ld, s_a, r_a, s_g, r_g, s_b, r_b, s_w, r_w, f_w, s_x, r_x,
    s_c, r_c, s_d, r_d, s_h, r_h, s_l, r_l, s_o, r_o, s_e, r_e, s_f, r_f, sem_o,
):
    me = lax.axis_index("ep")
    tp = lax.axis_index("tp")
    z = tp // 2
    c = tp % 2
    H = S // 2
    L = EP * CAP
    HS = EP // 2
    WIDTH = NZ * 256
    other = 1 - c
    partner = (me, 2 * z + other)
    home = me // HS
    own_half = home == c
    at_me = me - home * HS
    my_rows = pl.ds(pl.multiple_of(c * H, H), H)
    its_rows = pl.ds(pl.multiple_of(other * H, H), H)

    def zdev(d):
        return (me, 2 * ((z + d) % NZ) + c)

    def zcross(d):
        return (me, 2 * ((z + d) % NZ) + other)

    def zrel(rd):
        return (z + rd) % NZ

    def rows(j, rd):
        t = 2 * zrel(rd) + (c if j == 0 else other)
        return pl.multiple_of(t * 128, 128)

    def back_rel(d):
        return (NZ - d) % NZ

    far_first = sorted(range(1, NZ), key=lambda d: (-min(d, NZ - d), d))
    near_first = [0] + sorted(range(1, NZ), key=lambda d: (min(d, NZ - d), d))
    near = [rd for rd in near_first[1:] if min(rd, NZ - rd) <= NEAR]
    far = [rd for rd in near_first[1:] if min(rd, NZ - rd) > NEAR]

    def row(ref):
        return ref[...].astype(F32).reshape(1, 128)

    def wait(ref, sem):
        pltpu.make_async_copy(ref, ref, sem).wait()

    def send(src, dst, ssem, rsem, dev):
        pltpu.make_async_remote_copy(
            src_ref=src, dst_ref=dst, send_sem=ssem, recv_sem=rsem, device_id=dev, device_id_type=MESH
        ).start()

    loads = []

    def load(src, dst):
        k = len(loads)
        cp = pltpu.make_async_copy(src, dst, sem_ld.at[k])
        cp.start()
        loads.append(cp)
        return k

    k_tok = load(tok_h, tok_v)
    k_own = load(tok_h.at[my_rows], tok_a.at[0, 0])
    k_small = [
        load(a, b)
        for a, b in (
            (n1_h, n1_v), (n2_h, n2_v), (cb_h, cb_v), (rb_h, rb_v), (ib_h, ib_v), (dl_h, dl_v), (taps_h, taps_v)
        )
    ]
    k_rt = load(rt_h, rt_v)

    bar = pltpu.get_barrier_semaphore()

    def sig(dev):
        pl.semaphore_signal(bar, inc=1, device_id=dev, device_id_type=MESH)

    for d in range(1, NZ):
        sig(zdev(d))
        sig(zcross(d))
    sig(partner)

    def bar_ep(i, carry):
        e = (me + i) % EP
        sig((e, tp))
        sig((e, 2 * z + other))
        return carry

    lax.fori_loop(1, EP, bar_ep, 0)

    k_gr = load(grt_h, grt_v)
    k_er = load(ert_h, ert_v)
    k_conv = load(conv_h.at[:, my_rows], conv_p.at[0])
    k_convo = load(conv_h.at[1:3], conv_v)
    k_state = load(state_h.at[my_rows], state_p.at[0])
    k_bw = load(bw_h, bw_p.at[0])
    k_gw = load(gw_h, gw_p.at[0])
    k_rw = load(rw_h, rw_p.at[0])
    k_iw = load(iw_h, iw_p.at[0])
    k_ow = load(ow_h, ow_p.at[0])
    k_w = load(dn_h.at[:, pl.ds(pl.multiple_of(z * 256, 256), 256)], wdn.at[0, 0])
    k_g = load(gt_h, wcat.at[0])
    k_u = load(ut_h, wcat.at[2])

    loads[k_tok].wait()
    for k in k_small:
        loads[k].wait()
    gain_a[0, 0] = jnp.concatenate([row(n1_v), row(n2_v)], axis=0)
    par_v[0, 0:4] = jnp.concatenate([row(cb_v), row(rb_v), row(ib_v), row(dl_v)], axis=0)
    par_v[0, 4:8] = taps_v[...].astype(F32)

    pl.semaphore_wait(bar, 2 * (NZ - 1) + 1 + 2 * (EP - 1))

    for d in far_first:
        rd = back_rel(d)
        send(tok_v.at[my_rows], tok_a.at[rd, 0], s_a.at[d, 0], r_a.at[rd, 0], zdev(d))
        send(tok_v.at[its_rows], tok_a.at[rd, 1], s_a.at[d, 1], r_a.at[rd, 1], zcross(d))
        send(gain_a.at[0, 0], gain_a.at[rd, 0], s_g.at[d, 0], r_g.at[rd, 0], zdev(d))
        send(gain_a.at[0, 0], gain_a.at[rd, 1], s_g.at[d, 1], r_g.at[rd, 1], zcross(d))
    send(gain_a.at[0, 0], gain_a.at[0, 1], s_g.at[0, 1], r_g.at[0, 1], partner)
    send(tok_v.at[its_rows], tok_a.at[0, 1], s_a.at[0, 1], r_a.at[0, 1], partner)

    shared = []

    def share(src, dst):
        k = len(shared)
        send(src, dst, s_x.at[k], r_x.at[k], partner)
        shared.append(dst)
        return k

    x_bw = share(bw_h, bw_p.at[1])
    x_gw = share(gw_h, gw_p.at[1])
    x_par = share(par_v.at[0], par_v.at[1])
    x_conv = share(conv_h.at[:, its_rows], conv_p.at[1])
    x_rw = share(rw_h, rw_p.at[1])
    x_iw = share(iw_h, iw_p.at[1])
    x_state = share(state_h.at[its_rows], state_p.at[1])
    x_ow = share(ow_h, ow_p.at[1])
    x_g = share(gt_h, wcat.at[1])
    x_u = share(ut_h, wcat.at[3])

    def take(*ks):
        for k in ks:
            wait(shared[k], r_x.at[k])

    def send_down(dists):
        for d in dists:
            cols = pl.ds(pl.multiple_of(((z + d) % NZ) * 256, 256), 256)
            rd = back_rel(d)
            send(dn_h.at[:, cols], wdn.at[rd, 0], s_w.at[d], r_w.at[rd, 0], zdev(d))

    send_down([d for d in far_first if min(d, NZ - d) > 2])

    loads[k_rt].wait()
    loads[k_gr].wait()
    loads[k_er].wait()
    slot_row = lax.broadcasted_iota(jnp.int32, (L, S), 0)
    r0 = rt_v[0:1, :]
    r1 = rt_v[1:2, :]
    hit = ((slot_row // CAP) == r0) | ((slot_row // CAP) == r1)
    hit_f = jnp.where(hit, 1.0, 0.0)
    hit_b = hit_f.astype(BF16)
    before = jnp.where(
        lax.broadcasted_iota(jnp.int32, (S, S), 0) < lax.broadcasted_iota(jnp.int32, (S, S), 1), 1.0, 0.0
    ).astype(BF16)
    rank = mm(hit_b, before)
    sel = jnp.where(rank == (slot_row % CAP).astype(F32), hit_f, 0.0).astype(BF16)
    sel_v[...] = sel
    eye = jnp.where(
        lax.broadcasted_iota(jnp.int32, (S, S), 0) == lax.broadcasted_iota(jnp.int32, (S, S), 1), 1.0, 0.0
    ).astype(BF16)
    selt_v[0] = mm_nt(eye, sel)
    selt_v[1] = mm_nt(eye, hit_b)
    spread_e = jnp.where(
        lax.broadcasted_iota(jnp.int32, (L, EP), 0) // CAP == lax.broadcasted_iota(jnp.int32, (L, EP), 1), 1.0, 0.0
    ).astype(BF16)
    groups = grt_h.shape[0]
    spread_g = jnp.where(
        lax.broadcasted_iota(jnp.int32, (L, groups), 0) // (CAP * GS)
        == lax.broadcasted_iota(jnp.int32, (L, groups), 1),
        1.0,
        0.0,
    ).astype(BF16)
    for rd in range(NZ):
        cols = pl.ds(rows(0, rd), 128)
        rexp[rd, 0:L] = mm(spread_e, ert_v[:, cols]).astype(BF16)
        rexp[rd, L : 2 * L] = mm(spread_g, grt_v[:, cols]).astype(BF16)
    loads[k_conv].wait()
    loads[k_own].wait()
    take(x_par, x_conv)

    def par(i):
        return jnp.concatenate([par_v[0, i : i + 1, :], par_v[1, i : i + 1, :]], axis=1)

    conv_part = par(0) + sum(
        par(4 + j) * jnp.concatenate([conv_p[0, j], conv_p[1, j]], axis=1).astype(F32) for j in range(3)
    )
    loads[k_bw].wait()
    loads[k_gw].wait()
    take(x_bw, x_gw)

    def both(w_p, rd):
        i0 = pl.ds(rows(0, rd), 128)
        i1 = pl.ds(rows(1, rd), 128)
        return jnp.concatenate(
            [
                jnp.concatenate([w_p[0, i0, :], w_p[1, i0, :]], axis=1),
                jnp.concatenate([w_p[0, i1, :], w_p[1, i1, :]], axis=1),
            ],
            axis=0,
        )

    sums = [jnp.zeros((H, 128), F32), jnp.zeros((H, 256), F32), jnp.zeros((H, 256), F32)]
    for rd in near_first:
        parts = []
        for j in range(2):
            if (rd, j) != (0, 0):
                wait(gain_a.at[rd, j], r_g.at[rd, j])
                wait(tok_a.at[rd, j], r_a.at[rd, j])
            x = tok_a[rd, j].astype(F32)
            sums[0] = sums[0] + x * x
            parts.append((x * gain_a[rd, j][0:1, :]).astype(BF16))
        xg = jnp.concatenate(parts, axis=1)
        sums[1] = sums[1] + mm(xg, both(bw_p, rd))
        sums[2] = sums[2] + mm(xg, both(gw_p, rd))
    rstd = lax.rsqrt(jnp.sum(sums[0], axis=1, keepdims=True) / WIDTH + EPS)
    branch = (sums[1] * rstd).astype(BF16)
    gating = (sums[2] * rstd).astype(BF16).astype(F32)

    conv_out = conv_part + par(7) * branch.astype(F32)
    conv_low = conv_out.astype(BF16)
    loads[k_rw].wait()
    loads[k_iw].wait()
    loads[k_state].wait()
    take(x_rw, x_iw, x_state)

    def block_map(w_p):
        return jnp.concatenate([mm(conv_low[:, 0:128], w_p[0]), mm(conv_low[:, 128:256], w_p[1])], axis=1)

    recur_gate = sigmoid(block_map(rw_p) + par(1))
    input_gate = sigmoid(block_map(iw_p) + par(2))
    log_decay = 8.0 * recur_gate * log_sigmoid(par(3))
    state = jnp.concatenate([state_p[0], state_p[1]], axis=1)
    new_state = jnp.exp(log_decay) * state + jnp.sqrt(expm1_neg(2.0 * log_decay)) * (input_gate * conv_out)
    hid_b[0] = (new_state * gelu(gating)).astype(BF16)

    for d in far_first:
        rd = back_rel(d)
        send(hid_b.at[0], hid_b.at[rd], s_b.at[d], r_b.at[rd], zdev(d))
    nstate_v[my_rows, :] = new_state[:, 0:128]
    ns_x[...] = new_state[:, 128:256]
    branch_v[my_rows, :] = branch[:, 0:128]
    br_x[...] = branch[:, 128:256]
    send_down([d for d in far_first if min(d, NZ - d) <= 2])
    send(ns_x, nstate_v.at[my_rows], s_o.at[0], r_o.at[0], partner)
    send(br_x, branch_v.at[my_rows], s_o.at[1], r_o.at[1], partner)
    loads[k_convo].wait()
    out_conv = pltpu.make_async_copy(conv_v, nconv_h.at[0:2], sem_o.at[1])
    out_conv.start()
    loads[k_ow].wait()
    take(x_ow)
    proj = None
    for rd in near_first:
        if rd != 0:
            wait(hid_b.at[rd], r_b.at[rd])
        part = mm(hid_b[rd], both(ow_p, rd))
        proj = part if proj is None else proj + part
    resid = (jnp.concatenate([tok_a[0, 0], tok_a[0, 1]], axis=1).astype(F32) + proj).astype(BF16)
    res_c[0, c] = resid[:, 0:128]
    res_x[...] = resid[:, 128:256]

    send(res_x, res_c.at[0, c], s_c.at[0, 1], r_c.at[0, 1], partner)
    for d in far_first:
        rd = back_rel(d)
        send(res_c.at[0, c], res_c.at[rd, c], s_c.at[d, 0], r_c.at[rd, 0], zdev(d))
        send(res_x, res_c.at[rd, c], s_c.at[d, 1], r_c.at[rd, 1], zcross(d))

    def select(rd):
        return mm(sel_v[...], res_c[rd].reshape(S, 128)).astype(BF16).reshape(EP, CAP, 128)

    def dispatch(src, dst, ssem, rsem):
        def one(i, carry):
            e = (me + i) % EP
            send(src.at[e], dst.at[c * HS + at_me], ssem, rsem, (e, 2 * z + home))
            return carry

        lax.fori_loop(1, EP, one, 0)

        @pl.when(own_half)
        def _():
            dst[c * HS + at_me] = src[me]

        @pl.when(jnp.logical_not(own_half))
        def _():
            send(src.at[me], dst.at[c * HS + at_me], ssem, rsem, partner)

    def wait_blocks(ref, n_own, sem):
        @pl.when(n_own)
        def _():
            wait(ref.at[0 : EP - 1], sem)

        @pl.when(jnp.logical_not(n_own))
        def _():
            wait(ref, sem)

    wait(res_c.at[0, other], r_c.at[0, 1])
    ysel[...] = select(0)
    dispatch(ysel, xbuf.at[0], s_d.at[0], r_d.at[0])
    wait_blocks(xbuf.at[0], own_half, r_d.at[0])
    for rd in sorted(near, key=lambda d: -min(d, NZ - d)):
        send(xbuf.at[0], xbuf.at[rd], s_h.at[rd], r_h.at[rd], zdev(back_rel(rd)))
    for n, rd in enumerate(far):
        wait(res_c.at[rd, c], r_c.at[rd, 0])
        wait(res_c.at[rd, other], r_c.at[rd, 1])
        yfar[:, n] = select(rd)
    if far:
        dispatch(yfar, xfar, s_d.at[1], r_d.at[1])
    for rd in near:
        wait(res_c.at[rd, c], r_c.at[rd, 0])
        wait(res_c.at[rd, other], r_c.at[rd, 1])
    ss_row = jnp.zeros((S, 128), F32)
    for rd in near_first:
        xf = res_c[rd].reshape(S, 128).astype(F32)
        ss_row = ss_row + xf * xf
        xg = (xf * gain_a[rd, 0][1:2, :]).astype(BF16)
        part = mm_nt(xg, rexp[rd])
        if rd == 0:
            lg_own[...] = part
        else:
            lg_own[...] += part
    ss_own[...] = ss_row
    send(lg_own, lg_in, s_l.at[0], r_l.at[0], partner)
    send(ss_own, ss_in, s_l.at[1], r_l.at[1], partner)
    loads[k_w].wait()
    send(wdn.at[0, 0], wdn.at[0, 1], f_w.at[0], r_w.at[0, 1], partner)
    for rd in near_first[1:]:
        wait(wdn.at[rd, 0], r_w.at[rd, 0])
        send(wdn.at[rd, 0], wdn.at[rd, 1], f_w.at[rd], r_w.at[rd, 1], partner)
    wait(ns_x, r_o.at[0])
    wait(br_x, r_o.at[1])
    out_state = pltpu.make_async_copy(nstate_v, nstate_h, sem_o.at[0])
    out_state.start()
    out_branch = pltpu.make_async_copy(branch_v, nconv_h.at[2], sem_o.at[2])
    out_branch.start()

    loads[k_g].wait()
    loads[k_u].wait()
    take(x_g, x_u)

    def expert(n, rd, halves):
        parts = []
        for p in range(2):
            xf = halves[p].astype(F32)
            if n == 0 and p == 0:
                ssx_v[...] = xf * xf
            else:
                ssx_v[...] += xf * xf
            parts.append((xf * gain_a[rd, (p + c) % 2][1:2, :]).astype(BF16))
        cols = pl.ds(pl.multiple_of(zrel(rd) * 256, 256), 256)
        part = mm_nt(jnp.concatenate(parts, axis=1), wcat[:, :, cols].reshape(256, 256))
        if n == 0:
            acc_v[...] = part
        else:
            acc_v[...] += part

    def halves_of(ref):
        return [ref[p * HS : (p + 1) * HS].reshape(HS * CAP, 128) for p in range(2)]

    expert(0, 0, halves_of(xbuf.at[0]))
    if far:
        wait_blocks(xfar, own_half, r_d.at[1])
    for n, rd in enumerate(far):
        expert(1, rd, [xfar[p * HS : (p + 1) * HS, n].reshape(HS * CAP, 128) for p in range(2)])
    for rd in near:
        wait(xbuf.at[rd], r_h.at[rd])
        expert(1, rd, halves_of(xbuf.at[rd]))
    ss_slot = jnp.sum(ssx_v[...], axis=1, keepdims=True)
    gu = acc_v[...] * lax.rsqrt(ss_slot / WIDTH + EPS)
    gate = gu[:, 0:128]
    hid_e[0] = (gate * sigmoid(gate) * gu[:, 128:256]).astype(BF16)

    for d in far_first:
        rd = back_rel(d)
        send(hid_e.at[0], hid_e.at[rd], s_e.at[d], r_e.at[rd], zdev(d))

    wait(lg_in, r_l.at[0])
    wait(ss_in, r_l.at[1])
    ss_tot = jnp.sum(ss_own[...] + ss_in[...], axis=1, keepdims=True)
    rstd2 = lax.rsqrt(ss_tot / WIDTH + EPS)
    logits = (lg_own[...] + lg_in[...]) * rstd2
    e_exp = jnp.exp(logits[:, 0:L])
    g_exp = jnp.exp(logits[:, L : 2 * L])
    e_den = jnp.sum(e_exp * selt_v[1], axis=1, keepdims=True) * (1.0 / CAP)
    g_den = jnp.sum(g_exp, axis=1, keepdims=True) * (1.0 / (CAP * GS))
    combine = selt_v[0] * (g_exp / g_den) * (e_exp / e_den)
    comb_hi = combine.astype(BF16)
    comb_lo = (combine - comb_hi.astype(F32)).astype(BF16)
    for rd in range(NZ):
        wait(wdn.at[rd, 1], r_w.at[rd, 1])
    out = None
    for rd in near_first:
        if rd != 0:
            wait(hid_e.at[rd], r_e.at[rd])
        part = mm(hid_e[rd], wdn[rd].reshape(128, 256))
        out = part if out is None else out + part
    y = out.astype(BF16)
    y_v[0] = y[:, 0:128].reshape(HS, CAP, 128)
    y_v[1] = y[:, 128:256].reshape(HS, CAP, 128)

    def give_back(i, carry):
        s = c * HS + i

        @pl.when(s != me)
        def _():
            send(y_v.at[c, i], back_v.at[me], s_f.at[i, 0], r_f.at[0], (s, tp))

        send(y_v.at[other, i], back_v.at[me], s_f.at[i, 1], r_f.at[0], (s, 2 * z + other))
        return carry

    lax.fori_loop(0, HS, give_back, 0)

    @pl.when(own_half)
    def _():
        back_v[me] = y_v[c, at_me]

    wait_blocks(back_v, own_half, r_f.at[0])
    back = back_v[...].reshape(L, 128)
    moe = mm(comb_hi, back) + mm(comb_lo, back)
    mixed_v[...] = (res_c[0].reshape(S, 128).astype(F32) + moe).astype(BF16)
    out_mixed = pltpu.make_async_copy(mixed_v, mixed_h, sem_o.at[3])
    out_mixed.start()

    for d in range(1, NZ):
        for j in range(2):
            wait(gain_a.at[0, 0], s_g.at[d, j])
            wait(tok_a.at[0, 0], s_a.at[d, j])
            wait(res_x, s_c.at[d, j])
        wait(wdn.at[0, 0], s_w.at[d])
        wait(hid_b.at[0], s_b.at[d])
        wait(hid_e.at[0], s_e.at[d])
    for rd in range(NZ):
        wait(wdn.at[0, 0], f_w.at[rd])
    wait(gain_a.at[0, 0], s_g.at[0, 1])
    wait(tok_a.at[0, 0], s_a.at[0, 1])
    wait(res_x, s_c.at[0, 1])
    for k, dst in enumerate(shared):
        wait(dst, s_x.at[k])
    wait_blocks(ysel, own_half, s_d.at[0])
    if far:
        wait_blocks(yfar, own_half, s_d.at[1])
    for rd in near:
        wait(xbuf.at[0], s_h.at[rd])
    wait(ns_x, s_o.at[0])
    wait(br_x, s_o.at[1])
    wait(lg_own, s_l.at[0])
    wait(ss_own, s_l.at[1])

    def left(i, carry):
        @pl.when(c * HS + i != me)
        def _():
            wait(y_v.at[0, 0], s_f.at[i, 0])

        wait(y_v.at[0, 0], s_f.at[i, 1])
        return carry

    lax.fori_loop(0, HS, left, 0)
    out_state.wait()
    out_conv.wait()
    out_branch.wait()
    out_mixed.wait()


def emit(a_h, b_h, c_h, ao_h, bo_h, co_h, a_v, b_v, c_v, sem):
    trios = ((a_h, a_v, ao_h), (b_h, b_v, bo_h), (c_h, c_v, co_h))
    for k, (src, mid, _) in enumerate(trios):
        pltpu.make_async_copy(src, mid, sem.at[0, k]).start()
    for k, (src, mid, dst) in enumerate(trios):
        pltpu.make_async_copy(src, mid, sem.at[0, k]).wait()
        pltpu.make_async_copy(mid, dst, sem.at[1, k]).start()
    for k, (_, mid, dst) in enumerate(trios):
        pltpu.make_async_copy(mid, dst, sem.at[1, k]).wait()


def on_device(
    tokens, conv_state, recur_state, norm1_gain, branch_weight, gating_weight, conv_taps, conv_bias,
    recur_weight, recur_bias, input_weight, input_bias, decay_logit, out_weight, norm2_gain,
    group_router, expert_router, routes, gate_experts, up_experts, down_experts,
):
    EP = lax.axis_size("ep")
    TPN = lax.axis_size("tp")
    NZ = TPN // 2
    S = tokens.shape[0]
    CAP = 2 * routes.shape[1] * S // EP
    GS = expert_router.shape[1] // group_router.shape[1]
    L = EP * CAP
    args = (
        tokens,
        jnp.transpose(conv_state, (1, 0, 2)),
        recur_state,
        norm1_gain,
        norm2_gain,
        conv_bias,
        recur_bias,
        input_bias,
        decay_logit,
        conv_taps,
        branch_weight,
        gating_weight,
        recur_weight[0],
        input_weight[0],
        out_weight,
        group_router.T,
        expert_router.T,
        routes.T,
        gate_experts[0].T,
        up_experts[0].T,
        down_experts[0],
    )
    D = TPN * 128
    V = pltpu.VMEM
    dma = pltpu.SemaphoreType.DMA
    H = S // 2
    near_count = len([d for d in range(1, NZ) if min(d, NZ - d) <= NEAR])
    NF = max(NZ - 1 - near_count, 1)
    scratch = [
        V((S, 128), BF16),
        V((NZ, 2, H, 128), BF16),
        V((NZ, 2, 2, 128), F32),
        V((2, S, 128), BF16),
        V((2, 3, H, 128), BF16),
        V((2, H, 128), F32),
        V((128,), BF16), V((128,), BF16), V((128,), BF16),
        V((128,), F32), V((128,), F32), V((128,), F32),
        V((4, 128), BF16),
        V((2, 8, 128), F32),
        V((2, D, 128), BF16),
        V((2, D, 128), BF16),
        V((2, 128, 128), BF16),
        V((2, 128, 128), BF16),
        V((2, D, 128), BF16),
        V(group_router.T.shape, BF16),
        V(expert_router.T.shape, BF16),
        V((2, S), jnp.int32),
        V((4, 64, D), BF16),
        V((NZ, 2, 64, 256), BF16),
        V((NZ, H, 256), BF16),
        V((NZ, 2, H, 128), BF16),
        V((H, 128), BF16),
        V((EP, CAP, 128), BF16),
        V((EP, NF, CAP, 128), BF16),
        V((NZ, EP, CAP, 128), BF16),
        V((EP, NF, CAP, 128), BF16),
        V((NZ, 2 * L, 128), BF16),
        V((S, 2 * L), F32),
        V((S, 2 * L), F32),
        V((S, 128), F32),
        V((S, 128), F32),
        V((L // 2, 256), F32),
        V((L // 2, 128), F32),
        V((NZ, L // 2, 128), BF16),
        V((2, EP // 2, CAP, 128), BF16),
        V((EP, CAP, 128), BF16),
        V((S, 128), BF16),
        V((S, 128), F32),
        V((H, 128), F32),
        V((S, 128), BF16),
        V((H, 128), BF16),
        V((L, S), BF16),
        V((2, S, L), F32),
        dma((24,)),
        dma((NZ, 2)), dma((NZ, 2)),
        dma((NZ, 2)), dma((NZ, 2)),
        dma((NZ,)), dma((NZ,)),
        dma((NZ,)), dma((NZ, 2)), dma((NZ,)),
        dma((10,)), dma((10,)),
        dma((NZ, 2)), dma((NZ, 2)),
        dma((2,)), dma((2,)),
        dma((NZ,)), dma((NZ,)),
        dma((2,)), dma((2,)),
        dma((2,)), dma((2,)),
        dma((NZ,)), dma((NZ,)),
        dma((EP // 2, 2)), dma((1,)),
        dma((4,)),
    ]
    anyspace = pl.BlockSpec(memory_space=pl.ANY)
    mixed, new_state, new_conv = pl.pallas_call(
        functools.partial(kernel, EP, NZ, S, CAP, GS),
        out_shape=(
            jax.ShapeDtypeStruct((S, 128), BF16),
            jax.ShapeDtypeStruct((S, 128), F32),
            jax.ShapeDtypeStruct((3, S, 128), BF16),
        ),
        in_specs=[anyspace] * len(args),
        out_specs=[anyspace] * 3,
        scratch_shapes=scratch,
        compiler_params=pltpu.CompilerParams(
            collective_id=0, has_side_effects=True, vmem_limit_bytes=67_000_000
        ),
        name="layer",
    )(*args)
    shapes = ((S, 128), (S, 128), (3, S, 128))
    types = (BF16, F32, BF16)
    mixed, new_state, new_conv = pl.pallas_call(
        emit,
        out_shape=tuple(jax.ShapeDtypeStruct(a, b) for a, b in zip(shapes, types)),
        in_specs=[anyspace] * 3,
        out_specs=[anyspace] * 3,
        scratch_shapes=[V(a, b) for a, b in zip(shapes, types)] + [dma((2, 3))],
        name="emit",
    )(mixed, new_state, new_conv)
    return mixed, new_state, jnp.transpose(new_conv, (1, 0, 2))


def solution(mesh):
    return jax.shard_map(
        on_device,
        mesh=mesh,
        in_specs=(
            P("ep", "tp"),
            P("ep", None, "tp"),
            P("ep", "tp"),
            P("tp"),
            P(None, "tp"),
            P(None, "tp"),
            P(None, "tp"),
            P("tp"),
            P("tp", None, None),
            P("tp"),
            P("tp", None, None),
            P("tp"),
            P("tp"),
            P(None, "tp"),
            P("tp"),
            P(),
            P(),
            P("ep", None),
            P("ep", None, "tp"),
            P("ep", None, "tp"),
            P("ep", "tp", None),
        ),
        out_specs=(P("ep", "tp"), P("ep", "tp"), P("ep", None, "tp")),
        check_vma=False,
    )
```

time: 64.9 us -> 55.7 us (0.86)
  Pallas kernels: 61.5 us -> 54.8 us
  local copies, waits for them, and re-layouts: 2.59 us -> 0 us
    pallas_call x1, Pallas kernels: 61.5 us -> 53.3 us  [on_device(): pl.pallas_call(functools.partial(kernel, EP, NZ, S, CAP, GS), out_shape=(...]
    unnamed x7 -> x0, local copies, waits for them, and re-layouts: 2.59 us -> none
    pallas_call x0 -> x1, Pallas kernels: none -> 1.51 us  [on_device(): pl.pallas_call(emit, out_shape=tuple((jax.ShapeDtypeStruct(a, b) for a, b...]
where the time goes in v3:
time: 55.7 us; the launch traced here: 55.5 us
  Pallas kernels  54.8 us (98%)
  between operations  0.65 us (1%)
    pallas_call x1, Pallas kernels, on_device(): pl.pallas_call(functools.partial(kernel, EP, NZ, S, CAP, GS), out_shape=(...  53.3 us
    pallas_call x1, Pallas kernels, on_device(): pl.pallas_call(emit, out_shape=tuple((jax.ShapeDtypeStruct(a, b) for a, b...  1.51 us

profile of v3, /device:TPU:1, one launch (start us, length us, event | category | flops | bytes accessed | tf_op | source)
XLA Modules:
  0.0 55.5 jit_solution(3673347653815336022)
XLA Ops:
  0.6 53.3 %layer.1 = (bf16[64,128]{1,0:T(8,128)(2,1)}, f32[64,128]{1,0:T(8,128)}, bf16[3,64,128]{2,1,0:T(8,128)(2,1)}) custom-call(bf16[64,128]{1,0:T(8,128)(2,1)} %tok_h.1, bf16[3,64,128]{2,1,0:T(8,128)(2,1)} %bitcast.18, f32[64,128]{1,0:T(8,128)} %state_h.1, bf16[128]{0:T(256)(128)(2,1)} %n1_h.1, bf16[128]{0:T(256)(128)(2,1)} %n2_h.1, bf16[128]{0:T(256)(128)(2,1)} %cb_h.1, ...), custom_call_target="tpu_custom_call" | custom-call | tf_op jit(solution)/shard_map/layer/pallas_call | solution.py:641
  54.0 1.5 %emit.1 = (bf16[64,128]{1,0:T(8,128)(2,1)}, f32[64,128]{1,0:T(8,128)}, bf16[3,64,128]{2,1,0:T(8,128)(2,1)}) custom-call(bf16[64,128]{1,0:T(8,128)(2,1)} %get-tuple-element.9.a_h, f32[64,128]{1,0:T(8,128)} %get-tuple-element.10.b_h, bf16[3,64,128]{2,1,0:T(8,128)(2,1)} %get-tuple-element.11.c_h), custom_call_target="tpu_custom_call" | custom-call | tf_op jit(solution)/shard_map/emit/pallas_call | solution.py:658

commit v4 on v3

--- a/solution.py
+++ b/solution.py
@@ -9,6 +9,8 @@
 
 EPS = 1e-06
 NEAR = 2
+ENEAR = 2
+BATCH_AT = 3
 F32 = jnp.float32
 BF16 = jnp.bfloat16
 MESH = pl.DeviceIdType.MESH
@@ -52,11 +54,11 @@
     grt_h, ert_h, rt_h, gt_h, ut_h, dn_h,
     mixed_h, nstate_h, nconv_h,
     tok_v, tok_a, gain_a, conv_v, conv_p, state_p, n1_v, n2_v, cb_v, rb_v, ib_v, dl_v, taps_v, par_v,
-    bw_p, gw_p, rw_p, iw_p, ow_p, grt_v, ert_v, rt_v, wcat, wdn,
+    bw_p, gw_p, rw_p, iw_p, ow_p, grt_v, ert_v, rt_v, wcat, dnp, wdn,
     hid_b, res_c, res_x, ysel, yfar, xbuf, xfar, rexp, lg_own, lg_in, ss_own, ss_in, acc_v, ssx_v,
-    hid_e, y_v, back_v, mixed_v, nstate_v, ns_x, branch_v, br_x, sel_v, selt_v,
+    hid_e, y_v, yf_v, back_v, backf_v, moe_v, moe_in, mixed_v, nstate_v, ns_x, branch_v, br_x, sel_v, selt_v,
     sem_ld, s_a, r_a, s_g, r_g, s_b, r_b, s_w, r_w, f_w, s_x, r_x,
-    s_c, r_c, s_d, r_d, s_h, r_h, s_l, r_l, s_o, r_o, s_e, r_e, s_f, r_f, sem_o,
+    s_c, r_c, s_d, r_d, s_h, r_h, s_l, r_l, s_o, r_o, s_e, r_e, s_f, r_f, s_k, r_k, s_m, r_m, sem_o,
 ):
     me = lax.axis_index("ep")
     tp = lax.axis_index("tp")
@@ -94,6 +96,11 @@
     near_first = [0] + sorted(range(1, NZ), key=lambda d: (min(d, NZ - d), d))
     near = [rd for rd in near_first[1:] if min(rd, NZ - rd) <= NEAR]
     far = [rd for rd in near_first[1:] if min(rd, NZ - rd) > NEAR]
+    step = max(BATCH_AT, 1)
+    batches = [(lo, min(lo + step, len(far))) for lo in range(0, len(far), step)]
+
+    e_near = [rd for rd in near_first[1:] if min(rd, NZ - rd) <= ENEAR]
+    e_far = [rd for rd in near_first[1:] if min(rd, NZ - rd) > ENEAR]
 
     def row(ref):
         return ref[...].astype(F32).reshape(1, 128)
@@ -153,7 +160,7 @@
     k_rw = load(rw_h, rw_p.at[0])
     k_iw = load(iw_h, iw_p.at[0])
     k_ow = load(ow_h, ow_p.at[0])
-    k_w = load(dn_h.at[:, pl.ds(pl.multiple_of(z * 256, 256), 256)], wdn.at[0, 0])
+    k_w = load(dn_h, dnp.at[0])
     k_g = load(gt_h, wcat.at[0])
     k_u = load(ut_h, wcat.at[2])
 
@@ -190,9 +197,6 @@
     x_rw = share(rw_h, rw_p.at[1])
     x_iw = share(iw_h, iw_p.at[1])
     x_state = share(state_h.at[its_rows], state_p.at[1])
-    x_ow = share(ow_h, ow_p.at[1])
-    x_g = share(gt_h, wcat.at[1])
-    x_u = share(ut_h, wcat.at[3])
 
     def take(*ks):
         for k in ks:
@@ -204,7 +208,6 @@
             rd = back_rel(d)
             send(dn_h.at[:, cols], wdn.at[rd, 0], s_w.at[d], r_w.at[rd, 0], zdev(d))
 
-    send_down([d for d in far_first if min(d, NZ - d) > 2])
 
     loads[k_rt].wait()
     loads[k_gr].wait()
@@ -306,9 +309,10 @@
     ns_x[...] = new_state[:, 128:256]
     branch_v[my_rows, :] = branch[:, 0:128]
     br_x[...] = branch[:, 128:256]
-    send_down([d for d in far_first if min(d, NZ - d) <= 2])
+    send_down([d for d in far_first if min(d, NZ - d) in (1, 2)])
     send(ns_x, nstate_v.at[my_rows], s_o.at[0], r_o.at[0], partner)
     send(br_x, branch_v.at[my_rows], s_o.at[1], r_o.at[1], partner)
+    x_ow = share(ow_h, ow_p.at[1])
     loads[k_convo].wait()
     out_conv = pltpu.make_async_copy(conv_v, nconv_h.at[0:2], sem_o.at[1])
     out_conv.start()
@@ -330,46 +334,55 @@
         send(res_c.at[0, c], res_c.at[rd, c], s_c.at[d, 0], r_c.at[rd, 0], zdev(d))
         send(res_x, res_c.at[rd, c], s_c.at[d, 1], r_c.at[rd, 1], zcross(d))
 
+    x_g = share(gt_h, wcat.at[1])
+    x_u = share(ut_h, wcat.at[3])
+    x_dn = share(dn_h, dnp.at[1])
     def select(rd):
         return mm(sel_v[...], res_c[rd].reshape(S, 128)).astype(BF16).reshape(EP, CAP, 128)
 
-    def dispatch(src, dst, ssem, rsem):
+    def dispatch(src, dst, ssem, rsem, part=None):
+        slot = c * HS + at_me
+
+        def piece(ref, e):
+            return ref.at[e] if part is None else ref.at[e, part[0] : part[1]]
+
         def one(i, carry):
             e = (me + i) % EP
-            send(src.at[e], dst.at[c * HS + at_me], ssem, rsem, (e, 2 * z + home))
+            send(piece(src, e), piece(dst, slot), ssem, rsem, (e, 2 * z + home))
             return carry
 
         lax.fori_loop(1, EP, one, 0)
 
         @pl.when(own_half)
         def _():
-            dst[c * HS + at_me] = src[me]
+            piece(dst, slot)[...] = piece(src, me)[...]
 
         @pl.when(jnp.logical_not(own_half))
         def _():
-            send(src.at[me], dst.at[c * HS + at_me], ssem, rsem, partner)
-
-    def wait_blocks(ref, n_own, sem):
+            send(piece(src, me), piece(dst, slot), ssem, rsem, partner)
+
+    def wait_blocks(ref, n_own, sem, part=None):
         @pl.when(n_own)
         def _():
-            wait(ref.at[0 : EP - 1], sem)
+            wait(ref.at[0 : EP - 1] if part is None else ref.at[0 : EP - 1, part[0] : part[1]], sem)
 
         @pl.when(jnp.logical_not(n_own))
         def _():
-            wait(ref, sem)
+            wait(ref if part is None else ref.at[:, part[0] : part[1]], sem)
 
     wait(res_c.at[0, other], r_c.at[0, 1])
     ysel[...] = select(0)
     dispatch(ysel, xbuf.at[0], s_d.at[0], r_d.at[0])
+    for b, (lo, hi) in enumerate(batches):
+        for n in range(lo, hi):
+            rd = far[n]
+            wait(res_c.at[rd, c], r_c.at[rd, 0])
+            wait(res_c.at[rd, other], r_c.at[rd, 1])
+            yfar[:, n] = select(rd)
+        dispatch(yfar, xfar, s_d.at[1 + b], r_d.at[1 + b], (lo, hi))
     wait_blocks(xbuf.at[0], own_half, r_d.at[0])
     for rd in sorted(near, key=lambda d: -min(d, NZ - d)):
         send(xbuf.at[0], xbuf.at[rd], s_h.at[rd], r_h.at[rd], zdev(back_rel(rd)))
-    for n, rd in enumerate(far):
-        wait(res_c.at[rd, c], r_c.at[rd, 0])
-        wait(res_c.at[rd, other], r_c.at[rd, 1])
-        yfar[:, n] = select(rd)
-    if far:
-        dispatch(yfar, xfar, s_d.at[1], r_d.at[1])
     for rd in near:
         wait(res_c.at[rd, c], r_c.at[rd, 0])
         wait(res_c.at[rd, other], r_c.at[rd, 1])
@@ -386,9 +399,7 @@
     ss_own[...] = ss_row
     send(lg_own, lg_in, s_l.at[0], r_l.at[0], partner)
     send(ss_own, ss_in, s_l.at[1], r_l.at[1], partner)
-    loads[k_w].wait()
-    send(wdn.at[0, 0], wdn.at[0, 1], f_w.at[0], r_w.at[0, 1], partner)
-    for rd in near_first[1:]:
+    for rd in e_near:
         wait(wdn.at[rd, 0], r_w.at[rd, 0])
         send(wdn.at[rd, 0], wdn.at[rd, 1], f_w.at[rd], r_w.at[rd, 1], partner)
     wait(ns_x, r_o.at[0])
@@ -398,6 +409,18 @@
     out_branch = pltpu.make_async_copy(branch_v, nconv_h.at[2], sem_o.at[2])
     out_branch.start()
 
+    wait(lg_in, r_l.at[0])
+    wait(ss_in, r_l.at[1])
+    ss_tot = jnp.sum(ss_own[...] + ss_in[...], axis=1, keepdims=True)
+    rstd2 = lax.rsqrt(ss_tot / WIDTH + EPS)
+    logits = (lg_own[...] + lg_in[...]) * rstd2
+    e_exp = jnp.exp(logits[:, 0:L])
+    g_exp = jnp.exp(logits[:, L : 2 * L])
+    e_den = jnp.sum(e_exp * selt_v[1], axis=1, keepdims=True) * (1.0 / CAP)
+    g_den = jnp.sum(g_exp, axis=1, keepdims=True) * (1.0 / (CAP * GS))
+    combine = selt_v[0] * (g_exp / g_den) * (e_exp / e_den)
+    comb_hi = combine.astype(BF16)
+    comb_lo = (combine - comb_hi.astype(F32)).astype(BF16)
     loads[k_g].wait()
     loads[k_u].wait()
     take(x_g, x_u)
@@ -422,10 +445,10 @@
         return [ref[p * HS : (p + 1) * HS].reshape(HS * CAP, 128) for p in range(2)]
 
     expert(0, 0, halves_of(xbuf.at[0]))
-    if far:
-        wait_blocks(xfar, own_half, r_d.at[1])
-    for n, rd in enumerate(far):
-        expert(1, rd, [xfar[p * HS : (p + 1) * HS, n].reshape(HS * CAP, 128) for p in range(2)])
+    for b, (lo, hi) in enumerate(batches):
+        wait_blocks(xfar, own_half, r_d.at[1 + b], (lo, hi))
+        for n in range(lo, hi):
+            expert(1, far[n], [xfar[p * HS : (p + 1) * HS, n].reshape(HS * CAP, 128) for p in range(2)])
     for rd in near:
         wait(xbuf.at[rd], r_h.at[rd])
         expert(1, rd, halves_of(xbuf.at[rd]))
@@ -436,51 +459,63 @@
 
     for d in far_first:
         rd = back_rel(d)
-        send(hid_e.at[0], hid_e.at[rd], s_e.at[d], r_e.at[rd], zdev(d))
-
-    wait(lg_in, r_l.at[0])
-    wait(ss_in, r_l.at[1])
-    ss_tot = jnp.sum(ss_own[...] + ss_in[...], axis=1, keepdims=True)
-    rstd2 = lax.rsqrt(ss_tot / WIDTH + EPS)
-    logits = (lg_own[...] + lg_in[...]) * rstd2
-    e_exp = jnp.exp(logits[:, 0:L])
-    g_exp = jnp.exp(logits[:, L : 2 * L])
-    e_den = jnp.sum(e_exp * selt_v[1], axis=1, keepdims=True) * (1.0 / CAP)
-    g_den = jnp.sum(g_exp, axis=1, keepdims=True) * (1.0 / (CAP * GS))
-    combine = selt_v[0] * (g_exp / g_den) * (e_exp / e_den)
-    comb_hi = combine.astype(BF16)
-    comb_lo = (combine - comb_hi.astype(F32)).astype(BF16)
-    for rd in range(NZ):
+        if rd in e_near:
+            send(hid_e.at[0], hid_e.at[rd], s_e.at[d], r_e.at[rd], zdev(d))
+
+    def put(dst, y, at=()):
+        for p in range(2):
+            dst[(p, slice(None)) + at] = y[:, p * 128 : (p + 1) * 128].astype(BF16).reshape(HS, CAP, 128)
+
+    def give_back(src, dst, ssem, rsem):
+        def one(i, carry):
+            s = c * HS + i
+
+            @pl.when(s != me)
+            def _():
+                send(src.at[c, i], dst.at[me], ssem.at[i, 0], rsem, (s, tp))
+
+            send(src.at[other, i], dst.at[me], ssem.at[i, 1], rsem, (s, 2 * z + other))
+            return carry
+
+        lax.fori_loop(0, HS, one, 0)
+
+        @pl.when(own_half)
+        def _():
+            dst[me] = src[c, at_me]
+
+    def own_down(d):
+        cols = pl.ds(pl.multiple_of(zrel(d) * 256, 256), 256)
+        return dnp[:, :, cols].reshape(128, 256)
+
+    loads[k_w].wait()
+    take(x_dn)
+    for n, d in enumerate(e_far):
+        put(yf_v, mm(hid_e[0], own_down(d)), (n,))
+    if e_far:
+        give_back(yf_v, backf_v, s_k, r_k.at[0])
+    out = mm(hid_e[0], own_down(0))
+    for rd in e_near:
         wait(wdn.at[rd, 1], r_w.at[rd, 1])
-    out = None
-    for rd in near_first:
-        if rd != 0:
-            wait(hid_e.at[rd], r_e.at[rd])
-        part = mm(hid_e[rd], wdn[rd].reshape(128, 256))
-        out = part if out is None else out + part
-    y = out.astype(BF16)
-    y_v[0] = y[:, 0:128].reshape(HS, CAP, 128)
-    y_v[1] = y[:, 128:256].reshape(HS, CAP, 128)
-
-    def give_back(i, carry):
-        s = c * HS + i
-
-        @pl.when(s != me)
-        def _():
-            send(y_v.at[c, i], back_v.at[me], s_f.at[i, 0], r_f.at[0], (s, tp))
-
-        send(y_v.at[other, i], back_v.at[me], s_f.at[i, 1], r_f.at[0], (s, 2 * z + other))
-        return carry
-
-    lax.fori_loop(0, HS, give_back, 0)
-
-    @pl.when(own_half)
-    def _():
-        back_v[me] = y_v[c, at_me]
-
+        wait(hid_e.at[rd], r_e.at[rd])
+        out = out + mm(hid_e[rd], wdn[rd].reshape(128, 256))
+    put(y_v, out)
+
+    give_back(y_v, back_v, s_f, r_f.at[0])
+
+    def combined(back):
+        return mm(comb_hi, back) + mm(comb_lo, back)
+
+    if e_far:
+        wait_blocks(backf_v, own_half, r_k.at[0])
+    for n, d in sorted(enumerate(e_far), key=lambda p: -min(p[1], NZ - p[1])):
+        moe_v[d] = combined(backf_v[:, n].reshape(L, 128)).astype(BF16)
+        rd = back_rel(d)
+        send(moe_v.at[d], moe_in.at[rd], s_m.at[d], r_m.at[rd], zdev(d))
     wait_blocks(back_v, own_half, r_f.at[0])
-    back = back_v[...].reshape(L, 128)
-    moe = mm(comb_hi, back) + mm(comb_lo, back)
+    moe = combined(back_v[...].reshape(L, 128))
+    for rd in e_far:
+        wait(moe_in.at[rd], r_m.at[rd])
+        moe = moe + moe_in[rd].astype(F32)
     mixed_v[...] = (res_c[0].reshape(S, 128).astype(F32) + moe).astype(BF16)
     out_mixed = pltpu.make_async_copy(mixed_v, mixed_h, sem_o.at[3])
     out_mixed.start()
@@ -490,10 +525,13 @@
             wait(gain_a.at[0, 0], s_g.at[d, j])
             wait(tok_a.at[0, 0], s_a.at[d, j])
             wait(res_x, s_c.at[d, j])
-        wait(wdn.at[0, 0], s_w.at[d])
+        if min(d, NZ - d) <= ENEAR:
+            wait(wdn.at[0, 0], s_w.at[d])
+            wait(hid_e.at[0], s_e.at[d])
+        else:
+            wait(moe_v.at[d], s_m.at[d])
         wait(hid_b.at[0], s_b.at[d])
-        wait(hid_e.at[0], s_e.at[d])
-    for rd in range(NZ):
+    for rd in e_near:
         wait(wdn.at[0, 0], f_w.at[rd])
     wait(gain_a.at[0, 0], s_g.at[0, 1])
     wait(tok_a.at[0, 0], s_a.at[0, 1])
@@ -501,8 +539,8 @@
     for k, dst in enumerate(shared):
         wait(dst, s_x.at[k])
     wait_blocks(ysel, own_half, s_d.at[0])
-    if far:
-        wait_blocks(yfar, own_half, s_d.at[1])
+    for b, part in enumerate(batches):
+        wait_blocks(yfar, own_half, s_d.at[1 + b], part)
     for rd in near:
         wait(xbuf.at[0], s_h.at[rd])
     wait(ns_x, s_o.at[0])
@@ -514,8 +552,12 @@
         @pl.when(c * HS + i != me)
         def _():
             wait(y_v.at[0, 0], s_f.at[i, 0])
+            if e_far:
+                wait(yf_v.at[0, 0], s_k.at[i, 0])
 
         wait(y_v.at[0, 0], s_f.at[i, 1])
+        if e_far:
+            wait(yf_v.at[0, 0], s_k.at[i, 1])
         return carry
 
     lax.fori_loop(0, HS, left, 0)
@@ -577,6 +619,7 @@
     H = S // 2
     near_count = len([d for d in range(1, NZ) if min(d, NZ - d) <= NEAR])
     NF = max(NZ - 1 - near_count, 1)
+    NFE = max(len([d for d in range(1, NZ) if min(d, NZ - d) > ENEAR]), 1)
     scratch = [
         V((S, 128), BF16),
         V((NZ, 2, H, 128), BF16),
@@ -597,6 +640,7 @@
         V(expert_router.T.shape, BF16),
         V((2, S), jnp.int32),
         V((4, 64, D), BF16),
+        V((2, 64, D), BF16),
         V((NZ, 2, 64, 256), BF16),
         V((NZ, H, 256), BF16),
         V((NZ, 2, H, 128), BF16),
@@ -614,7 +658,11 @@
         V((L // 2, 128), F32),
         V((NZ, L // 2, 128), BF16),
         V((2, EP // 2, CAP, 128), BF16),
+        V((2, EP // 2, NFE, CAP, 128), BF16),
         V((EP, CAP, 128), BF16),
+        V((EP, NFE, CAP, 128), BF16),
+        V((NZ, S, 128), BF16),
+        V((NZ, S, 128), BF16),
         V((S, 128), BF16),
         V((S, 128), F32),
         V((H, 128), F32),
@@ -627,14 +675,16 @@
         dma((NZ, 2)), dma((NZ, 2)),
         dma((NZ,)), dma((NZ,)),
         dma((NZ,)), dma((NZ, 2)), dma((NZ,)),
-        dma((10,)), dma((10,)),
+        dma((11,)), dma((11,)),
         dma((NZ, 2)), dma((NZ, 2)),
-        dma((2,)), dma((2,)),
+        dma((NZ,)), dma((NZ,)),
         dma((NZ,)), dma((NZ,)),
         dma((2,)), dma((2,)),
         dma((2,)), dma((2,)),
         dma((NZ,)), dma((NZ,)),
         dma((EP // 2, 2)), dma((1,)),
+        dma((EP // 2, 2)), dma((1,)),
+        dma((NZ,)), dma((NZ,)),
         dma((4,)),
     ]
     anyspace = pl.BlockSpec(memory_space=pl.ANY)

time: 55.7 us -> 51.4 us (0.923)
  Pallas kernels: 54.8 us -> 50.4 us
    pallas_call x1, Pallas kernels: 53.3 us -> 48.9 us  [on_device(): pl.pallas_call(functools.partial(kernel, EP, NZ, S, CAP, GS), out_shape=(...]
where the time goes in v4:
time: 51.4 us; the launch traced here: 51.1 us
  Pallas kernels  50.4 us (98%)
  between operations  0.65 us (1%)
    pallas_call x1, Pallas kernels, on_device(): pl.pallas_call(functools.partial(kernel, EP, NZ, S, CAP, GS), out_shape=(...  48.9 us
    pallas_call x1, Pallas kernels, on_device(): pl.pallas_call(emit, out_shape=tuple((jax.ShapeDtypeStruct(a, b) for a, b...  1.51 us

profile of v4, /device:TPU:1, one launch (start us, length us, event | category | flops | bytes accessed | tf_op | source)
XLA Modules:
  0.0 51.1 jit_solution(13354888544770025887)
XLA Ops:
  0.6 48.9 %layer.1 = (bf16[64,128]{1,0:T(8,128)(2,1)}, f32[64,128]{1,0:T(8,128)}, bf16[3,64,128]{2,1,0:T(8,128)(2,1)}) custom-call(bf16[64,128]{1,0:T(8,128)(2,1)} %tok_h.1, bf16[3,64,128]{2,1,0:T(8,128)(2,1)} %bitcast.18, f32[64,128]{1,0:T(8,128)} %state_h.1, bf16[128]{0:T(256)(128)(2,1)} %n1_h.1, bf16[128]{0:T(256)(128)(2,1)} %n2_h.1, bf16[128]{0:T(256)(128)(2,1)} %cb_h.1, ...), custom_call_target="tpu_custom_call" | custom-call | tf_op jit(solution)/shard_map/layer/pallas_call | solution.py:691
  49.6 1.5 %emit.1 = (bf16[64,128]{1,0:T(8,128)(2,1)}, f32[64,128]{1,0:T(8,128)}, bf16[3,64,128]{2,1,0:T(8,128)(2,1)}) custom-call(bf16[64,128]{1,0:T(8,128)(2,1)} %get-tuple-element.9.a_h, f32[64,128]{1,0:T(8,128)} %get-tuple-element.10.b_h, bf16[3,64,128]{2,1,0:T(8,128)(2,1)} %get-tuple-element.11.c_h), custom_call_target="tpu_custom_call" | custom-call | tf_op jit(solution)/shard_map/emit/pallas_call | solution.py:708

commit v5 on v4

--- a/solution.py
+++ b/solution.py
@@ -52,13 +52,13 @@
     EP, NZ, S, CAP, GS,
     tok_h, conv_h, state_h, n1_h, n2_h, cb_h, rb_h, ib_h, dl_h, taps_h, bw_h, gw_h, rw_h, iw_h, ow_h,
     grt_h, ert_h, rt_h, gt_h, ut_h, dn_h,
-    mixed_h, nstate_h, nconv_h,
+    mixed_o, nstate_o, nconv_o,
     tok_v, tok_a, gain_a, conv_v, conv_p, state_p, n1_v, n2_v, cb_v, rb_v, ib_v, dl_v, taps_v, par_v,
     bw_p, gw_p, rw_p, iw_p, ow_p, grt_v, ert_v, rt_v, wcat, dnp, wdn,
-    hid_b, res_c, res_x, ysel, yfar, xbuf, xfar, rexp, lg_own, lg_in, ss_own, ss_in, acc_v, ssx_v,
-    hid_e, y_v, yf_v, back_v, backf_v, moe_v, moe_in, mixed_v, nstate_v, ns_x, branch_v, br_x, sel_v, selt_v,
+    hid_b, res_c, res_x, ysel, yfar, xown, xbuf, xfar, rexp, lg_own, lg_in, ss_own, ss_in, acc_v, ssx_v,
+    hid_e, y_v, yf_v, back_v, backf_v, moe_v, moe_in, nstate_v, ns_x, branch_v, br_x, sel_v, selh_v, selt_v,
     sem_ld, s_a, r_a, s_g, r_g, s_b, r_b, s_w, r_w, f_w, s_x, r_x,
-    s_c, r_c, s_d, r_d, s_h, r_h, s_l, r_l, s_o, r_o, s_e, r_e, s_f, r_f, s_k, r_k, s_m, r_m, sem_o,
+    s_c, r_c, s_d, r_d, s_h, r_h, s_l, r_l, s_o, r_o, s_e, r_e, s_f, r_f, s_k, r_k, s_m, r_m,
 ):
     me = lax.axis_index("ep")
     tp = lax.axis_index("tp")
@@ -113,6 +113,24 @@
             src_ref=src, dst_ref=dst, send_sem=ssem, recv_sem=rsem, device_id=dev, device_id_type=MESH
         ).start()
 
+    bar = pltpu.get_barrier_semaphore()
+
+    def sig(dev):
+        pl.semaphore_signal(bar, inc=1, device_id=dev, device_id_type=MESH)
+
+    for d in range(1, NZ):
+        sig(zdev(d))
+        sig(zcross(d))
+    sig(partner)
+
+    def bar_ep(i, carry):
+        e = (me + i) % EP
+        sig((e, tp))
+        sig((e, 2 * z + other))
+        return carry
+
+    lax.fori_loop(1, EP, bar_ep, 0, unroll=True)
+
     loads = []
 
     def load(src, dst):
@@ -131,24 +149,6 @@
         )
     ]
     k_rt = load(rt_h, rt_v)
-
-    bar = pltpu.get_barrier_semaphore()
-
-    def sig(dev):
-        pl.semaphore_signal(bar, inc=1, device_id=dev, device_id_type=MESH)
-
-    for d in range(1, NZ):
-        sig(zdev(d))
-        sig(zcross(d))
-    sig(partner)
-
-    def bar_ep(i, carry):
-        e = (me + i) % EP
-        sig((e, tp))
-        sig((e, 2 * z + other))
-        return carry
-
-    lax.fori_loop(1, EP, bar_ep, 0)
 
     k_gr = load(grt_h, grt_v)
     k_er = load(ert_h, ert_v)
@@ -175,10 +175,12 @@
 
     for d in far_first:
         rd = back_rel(d)
+        send(gain_a.at[0, 0], gain_a.at[rd, 0], s_g.at[d, 0], r_g.at[rd, 0], zdev(d))
+        send(gain_a.at[0, 0], gain_a.at[rd, 1], s_g.at[d, 1], r_g.at[rd, 1], zcross(d))
+    for d in far_first:
+        rd = back_rel(d)
         send(tok_v.at[my_rows], tok_a.at[rd, 0], s_a.at[d, 0], r_a.at[rd, 0], zdev(d))
         send(tok_v.at[its_rows], tok_a.at[rd, 1], s_a.at[d, 1], r_a.at[rd, 1], zcross(d))
-        send(gain_a.at[0, 0], gain_a.at[rd, 0], s_g.at[d, 0], r_g.at[rd, 0], zdev(d))
-        send(gain_a.at[0, 0], gain_a.at[rd, 1], s_g.at[d, 1], r_g.at[rd, 1], zcross(d))
     send(gain_a.at[0, 0], gain_a.at[0, 1], s_g.at[0, 1], r_g.at[0, 1], partner)
     send(tok_v.at[its_rows], tok_a.at[0, 1], s_a.at[0, 1], r_a.at[0, 1], partner)
 
@@ -224,6 +226,10 @@
     rank = mm(hit_b, before)
     sel = jnp.where(rank == (slot_row % CAP).astype(F32), hit_f, 0.0).astype(BF16)
     sel_v[...] = sel
+    pick = jnp.where(
+        lax.broadcasted_iota(jnp.int32, (S, H), 0) == lax.broadcasted_iota(jnp.int32, (S, H), 1) + c * H, 1.0, 0.0
+    ).astype(BF16)
+    selh_v[...] = mm(sel, pick).astype(BF16)
     eye = jnp.where(
         lax.broadcasted_iota(jnp.int32, (S, S), 0) == lax.broadcasted_iota(jnp.int32, (S, S), 1), 1.0, 0.0
     ).astype(BF16)
@@ -314,8 +320,7 @@
     send(br_x, branch_v.at[my_rows], s_o.at[1], r_o.at[1], partner)
     x_ow = share(ow_h, ow_p.at[1])
     loads[k_convo].wait()
-    out_conv = pltpu.make_async_copy(conv_v, nconv_h.at[0:2], sem_o.at[1])
-    out_conv.start()
+    nconv_o[0:2] = conv_v[...]
     loads[k_ow].wait()
     take(x_ow)
     proj = None
@@ -337,9 +342,6 @@
     x_g = share(gt_h, wcat.at[1])
     x_u = share(ut_h, wcat.at[3])
     x_dn = share(dn_h, dnp.at[1])
-    def select(rd):
-        return mm(sel_v[...], res_c[rd].reshape(S, 128)).astype(BF16).reshape(EP, CAP, 128)
-
     def dispatch(src, dst, ssem, rsem, part=None):
         slot = c * HS + at_me
 
@@ -351,7 +353,7 @@
             send(piece(src, e), piece(dst, slot), ssem, rsem, (e, 2 * z + home))
             return carry
 
-        lax.fori_loop(1, EP, one, 0)
+        lax.fori_loop(1, EP, one, 0, unroll=True)
 
         @pl.when(own_half)
         def _():
@@ -370,19 +372,26 @@
         def _():
             wait(ref if part is None else ref.at[:, part[0] : part[1]], sem)
 
-    wait(res_c.at[0, other], r_c.at[0, 1])
-    ysel[...] = select(0)
-    dispatch(ysel, xbuf.at[0], s_d.at[0], r_d.at[0])
+    for j in range(2):
+        half = mm(selh_v[...], resid[:, j * 128 : (j + 1) * 128]).astype(BF16)
+        ysel[:, c if j == 0 else other] = half.reshape(EP, CAP, 128)
+    dispatch(ysel, xown, s_d.at[0], r_d.at[0])
+    wait_blocks(xown, own_half, r_d.at[0])
+    for p in range(2):
+        xbuf[0, p * HS : (p + 1) * HS] = xown[0:HS, p] + xown[HS : 2 * HS, p]
+    for rd in sorted(near, key=lambda d: -min(d, NZ - d)):
+        send(xbuf.at[0], xbuf.at[rd], s_h.at[rd], r_h.at[rd], zdev(back_rel(rd)))
     for b, (lo, hi) in enumerate(batches):
         for n in range(lo, hi):
             rd = far[n]
             wait(res_c.at[rd, c], r_c.at[rd, 0])
             wait(res_c.at[rd, other], r_c.at[rd, 1])
-            yfar[:, n] = select(rd)
+        chunks = jnp.concatenate([res_c[far[n]].reshape(S, 128) for n in range(lo, hi)], axis=1)
+        rows_out = mm(sel_v[...], chunks).astype(BF16)
+        for n in range(lo, hi):
+            yfar[:, n] = rows_out[:, (n - lo) * 128 : (n - lo + 1) * 128].reshape(EP, CAP, 128)
         dispatch(yfar, xfar, s_d.at[1 + b], r_d.at[1 + b], (lo, hi))
-    wait_blocks(xbuf.at[0], own_half, r_d.at[0])
-    for rd in sorted(near, key=lambda d: -min(d, NZ - d)):
-        send(xbuf.at[0], xbuf.at[rd], s_h.at[rd], r_h.at[rd], zdev(back_rel(rd)))
+    wait(res_c.at[0, other], r_c.at[0, 1])
     for rd in near:
         wait(res_c.at[rd, c], r_c.at[rd, 0])
         wait(res_c.at[rd, other], r_c.at[rd, 1])
@@ -404,10 +413,8 @@
         send(wdn.at[rd, 0], wdn.at[rd, 1], f_w.at[rd], r_w.at[rd, 1], partner)
     wait(ns_x, r_o.at[0])
     wait(br_x, r_o.at[1])
-    out_state = pltpu.make_async_copy(nstate_v, nstate_h, sem_o.at[0])
-    out_state.start()
-    out_branch = pltpu.make_async_copy(branch_v, nconv_h.at[2], sem_o.at[2])
-    out_branch.start()
+    nstate_o[...] = nstate_v[...]
+    nconv_o[2] = branch_v[...]
 
     wait(lg_in, r_l.at[0])
     wait(ss_in, r_l.at[1])
@@ -421,22 +428,24 @@
     combine = selt_v[0] * (g_exp / g_den) * (e_exp / e_den)
     comb_hi = combine.astype(BF16)
     comb_lo = (combine - comb_hi.astype(F32)).astype(BF16)
+    comb = jnp.concatenate([comb_hi, comb_lo], axis=0)
     loads[k_g].wait()
     loads[k_u].wait()
     take(x_g, x_u)
 
-    def expert(n, rd, halves):
-        parts = []
-        for p in range(2):
-            xf = halves[p].astype(F32)
-            if n == 0 and p == 0:
-                ssx_v[...] = xf * xf
-            else:
-                ssx_v[...] += xf * xf
-            parts.append((xf * gain_a[rd, (p + c) % 2][1:2, :]).astype(BF16))
-        cols = pl.ds(pl.multiple_of(zrel(rd) * 256, 256), 256)
-        part = mm_nt(jnp.concatenate(parts, axis=1), wcat[:, :, cols].reshape(256, 256))
-        if n == 0:
+    def expert(first, chunks):
+        squares = None if first else ssx_v[...]
+        parts, weights = [], []
+        for rd, halves in chunks:
+            for p in range(2):
+                xf = halves[p].astype(F32)
+                squares = xf * xf if squares is None else squares + xf * xf
+                parts.append((xf * gain_a[rd, (p + c) % 2][1:2, :]).astype(BF16))
+            cols = pl.ds(pl.multiple_of(zrel(rd) * 256, 256), 256)
+            weights.append(wcat[:, :, cols].reshape(256, 256))
+        ssx_v[...] = squares
+        part = mm_nt(jnp.concatenate(parts, axis=1), jnp.concatenate(weights, axis=1))
+        if first:
             acc_v[...] = part
         else:
             acc_v[...] += part
@@ -444,14 +453,20 @@
     def halves_of(ref):
         return [ref[p * HS : (p + 1) * HS].reshape(HS * CAP, 128) for p in range(2)]
 
-    expert(0, 0, halves_of(xbuf.at[0]))
+    expert(True, [(0, halves_of(xbuf.at[0]))])
     for b, (lo, hi) in enumerate(batches):
         wait_blocks(xfar, own_half, r_d.at[1 + b], (lo, hi))
-        for n in range(lo, hi):
-            expert(1, far[n], [xfar[p * HS : (p + 1) * HS, n].reshape(HS * CAP, 128) for p in range(2)])
+        expert(
+            False,
+            [
+                (far[n], [xfar[p * HS : (p + 1) * HS, n].reshape(HS * CAP, 128) for p in range(2)])
+                for n in range(lo, hi)
+            ],
+        )
     for rd in near:
         wait(xbuf.at[rd], r_h.at[rd])
-        expert(1, rd, halves_of(xbuf.at[rd]))
+    if near:
+        expert(False, [(rd, halves_of(xbuf.at[rd])) for rd in near])
     ss_slot = jnp.sum(ssx_v[...], axis=1, keepdims=True)
     gu = acc_v[...] * lax.rsqrt(ss_slot / WIDTH + EPS)
     gate = gu[:, 0:128]
@@ -477,7 +492,7 @@
             send(src.at[other, i], dst.at[me], ssem.at[i, 1], rsem, (s, 2 * z + other))
             return carry
 
-        lax.fori_loop(0, HS, one, 0)
+        lax.fori_loop(0, HS, one, 0, unroll=True)
 
         @pl.when(own_half)
         def _():
@@ -503,23 +518,16 @@
     give_back(y_v, back_v, s_f, r_f.at[0])
 
     def combined(back):
-        return mm(comb_hi, back) + mm(comb_lo, back)
+        pair = mm(comb, back)
+        return pair[0:S] + pair[S : 2 * S]
 
     if e_far:
         wait_blocks(backf_v, own_half, r_k.at[0])
+        parts = combined(jnp.concatenate([backf_v[:, n].reshape(L, 128) for n in range(len(e_far))], axis=1))
     for n, d in sorted(enumerate(e_far), key=lambda p: -min(p[1], NZ - p[1])):
-        moe_v[d] = combined(backf_v[:, n].reshape(L, 128)).astype(BF16)
+        moe_v[d] = parts[:, n * 128 : (n + 1) * 128].astype(BF16)
         rd = back_rel(d)
         send(moe_v.at[d], moe_in.at[rd], s_m.at[d], r_m.at[rd], zdev(d))
-    wait_blocks(back_v, own_half, r_f.at[0])
-    moe = combined(back_v[...].reshape(L, 128))
-    for rd in e_far:
-        wait(moe_in.at[rd], r_m.at[rd])
-        moe = moe + moe_in[rd].astype(F32)
-    mixed_v[...] = (res_c[0].reshape(S, 128).astype(F32) + moe).astype(BF16)
-    out_mixed = pltpu.make_async_copy(mixed_v, mixed_h, sem_o.at[3])
-    out_mixed.start()
-
     for d in range(1, NZ):
         for j in range(2):
             wait(gain_a.at[0, 0], s_g.at[d, j])
@@ -561,21 +569,23 @@
         return carry
 
     lax.fori_loop(0, HS, left, 0)
-    out_state.wait()
-    out_conv.wait()
-    out_branch.wait()
-    out_mixed.wait()
-
-
-def emit(a_h, b_h, c_h, ao_h, bo_h, co_h, a_v, b_v, c_v, sem):
-    trios = ((a_h, a_v, ao_h), (b_h, b_v, bo_h), (c_h, c_v, co_h))
-    for k, (src, mid, _) in enumerate(trios):
-        pltpu.make_async_copy(src, mid, sem.at[0, k]).start()
-    for k, (src, mid, dst) in enumerate(trios):
-        pltpu.make_async_copy(src, mid, sem.at[0, k]).wait()
-        pltpu.make_async_copy(mid, dst, sem.at[1, k]).start()
-    for k, (_, mid, dst) in enumerate(trios):
-        pltpu.make_async_copy(mid, dst, sem.at[1, k]).wait()
+    wait_blocks(back_v, own_half, r_f.at[0])
+    moe = combined(back_v[...].reshape(L, 128))
+    for rd in e_far:
+        wait(moe_in.at[rd], r_m.at[rd])
+        moe = moe + moe_in[rd].astype(F32)
+    mixed_o[...] = (res_c[0].reshape(S, 128).astype(F32) + moe).astype(BF16)
+
+
+def emit(a_v, b_v, c_v, ao_h, bo_h, co_h, sem):
+    copies = [
+        pltpu.make_async_copy(src, dst, sem.at[k])
+        for k, (src, dst) in enumerate(((a_v, ao_h), (b_v, bo_h), (c_v, co_h)))
+    ]
+    for copy in copies:
+        copy.start()
+    for copy in copies:
+        copy.wait()
 
 
 def on_device(
@@ -645,8 +655,9 @@
         V((NZ, H, 256), BF16),
         V((NZ, 2, H, 128), BF16),
         V((H, 128), BF16),
-        V((EP, CAP, 128), BF16),
+        V((EP, 2, CAP, 128), BF16),
         V((EP, NF, CAP, 128), BF16),
+        V((EP, 2, CAP, 128), BF16),
         V((NZ, EP, CAP, 128), BF16),
         V((EP, NF, CAP, 128), BF16),
         V((NZ, 2 * L, 128), BF16),
@@ -663,12 +674,12 @@
         V((EP, NFE, CAP, 128), BF16),
         V((NZ, S, 128), BF16),
         V((NZ, S, 128), BF16),
-        V((S, 128), BF16),
         V((S, 128), F32),
         V((H, 128), F32),
         V((S, 128), BF16),
         V((H, 128), BF16),
         V((L, S), BF16),
+        V((L, H), BF16),
         V((2, S, L), F32),
         dma((24,)),
         dma((NZ, 2)), dma((NZ, 2)),
@@ -685,21 +696,20 @@
         dma((EP // 2, 2)), dma((1,)),
         dma((EP // 2, 2)), dma((1,)),
         dma((NZ,)), dma((NZ,)),
-        dma((4,)),
     ]
     anyspace = pl.BlockSpec(memory_space=pl.ANY)
     mixed, new_state, new_conv = pl.pallas_call(
         functools.partial(kernel, EP, NZ, S, CAP, GS),
         out_shape=(
-            jax.ShapeDtypeStruct((S, 128), BF16),
-            jax.ShapeDtypeStruct((S, 128), F32),
-            jax.ShapeDtypeStruct((3, S, 128), BF16),
+            V((S, 128), BF16),
+            V((S, 128), F32),
+            V((3, S, 128), BF16),
         ),
         in_specs=[anyspace] * len(args),
-        out_specs=[anyspace] * 3,
+        out_specs=[pl.BlockSpec(memory_space=pltpu.VMEM)] * 3,
         scratch_shapes=scratch,
         compiler_params=pltpu.CompilerParams(
-            collective_id=0, has_side_effects=True, vmem_limit_bytes=67_000_000
+            collective_id=0, has_side_effects=True, vmem_limit_bytes=57000000
         ),
         name="layer",
     )(*args)
@@ -708,9 +718,10 @@
     mixed, new_state, new_conv = pl.pallas_call(
         emit,
         out_shape=tuple(jax.ShapeDtypeStruct(a, b) for a, b in zip(shapes, types)),
-        in_specs=[anyspace] * 3,
+        in_specs=[pl.BlockSpec(memory_space=pltpu.VMEM)] * 3,
         out_specs=[anyspace] * 3,
-        scratch_shapes=[V(a, b) for a, b in zip(shapes, types)] + [dma((2, 3))],
+        scratch_shapes=[dma((3,))],
+        compiler_params=pltpu.CompilerParams(vmem_limit_bytes=2 * 1024 * 1024),
         name="emit",
     )(mixed, new_state, new_conv)
     return mixed, new_state, jnp.transpose(new_conv, (1, 0, 2))

time: 51.4 us -> 49.4 us (0.961)
  Pallas kernels: 50.4 us -> 48.6 us
    pallas_call x1, Pallas kernels: 48.9 us -> 47.9 us  [on_device(): pl.pallas_call(functools.partial(kernel, EP, NZ, S, CAP, GS), out_shape=(...]
    pallas_call x1, Pallas kernels: 1.51 us -> 0.67 us  [on_device(): pl.pallas_call(emit, out_shape=tuple((jax.ShapeDtypeStruct(a, b) for a, b...]
where the time goes in v5:
time: 49.4 us; the launch traced here: 49.3 us
  Pallas kernels  48.6 us (98%)
  between operations  0.65 us (1%)
    pallas_call x1, Pallas kernels, on_device(): pl.pallas_call(functools.partial(kernel, EP, NZ, S, CAP, GS), out_shape=(...  47.9 us

profile of v5, /device:TPU:1, one launch (start us, length us, event | category | flops | bytes accessed | tf_op | source)
XLA Modules:
  0.0 49.3 jit_solution(10269054716807961788)
XLA Ops:
  0.6 47.9 %layer.1 = (bf16[64,128]{1,0:T(8,128)(2,1)S(1)}, f32[64,128]{1,0:T(8,128)S(1)}, bf16[3,64,128]{2,1,0:T(8,128)(2,1)S(1)}) custom-call(bf16[64,128]{1,0:T(8,128)(2,1)} %tok_h.1, bf16[3,64,128]{2,1,0:T(8,128)(2,1)} %bitcast.18, f32[64,128]{1,0:T(8,128)} %state_h.1, bf16[128]{0:T(256)(128)(2,1)} %n1_h.1, bf16[128]{0:T(256)(128)(2,1)} %n2_h.1, ...), custom_call_target="tpu_custom_call" | custom-call | tf_op jit(solution)/shard_map/layer/pallas_call | solution.py:701
  48.6 0.7 %emit.1 = (bf16[64,128]{1,0:T(8,128)(2,1)}, f32[64,128]{1,0:T(8,128)}, bf16[3,64,128]{2,1,0:T(8,128)(2,1)}) custom-call(bf16[64,128]{1,0:T(8,128)(2,1)S(1)} %get-tuple-element.9.a_v, f32[64,128]{1,0:T(8,128)S(1)} %get-tuple-element.10.b_v, bf16[3,64,128]{2,1,0:T(8,128)(2,1)S(1)} %get-tuple-element.11.c_v), custom_call_target="tpu_custom_call" | custom-call | tf_op jit(solution)/shard_map/emit/pallas_call | solution.py:718

commit v6 on v5

--- a/solution.py
+++ b/solution.py
@@ -8,9 +8,8 @@
 from jax.sharding import PartitionSpec as P
 
 EPS = 1e-06
-NEAR = 2
 ENEAR = 2
-BATCH_AT = 3
+BATCH_AT = 4
 F32 = jnp.float32
 BF16 = jnp.bfloat16
 MESH = pl.DeviceIdType.MESH
@@ -94,8 +93,12 @@
 
     far_first = sorted(range(1, NZ), key=lambda d: (-min(d, NZ - d), d))
     near_first = [0] + sorted(range(1, NZ), key=lambda d: (min(d, NZ - d), d))
-    near = [rd for rd in near_first[1:] if min(rd, NZ - rd) <= NEAR]
-    far = [rd for rd in near_first[1:] if min(rd, NZ - rd) > NEAR]
+    near = [rd for rd in near_first[1:] if min(rd, NZ - rd) <= 1]
+    far = [rd for rd in near_first[1:] if min(rd, NZ - rd) > 1]
+    if NZ > 4:
+        by_parity = 2 + (z % 2) * (NZ - 4)
+        near = [by_parity] + near
+        far = [NZ - by_parity] + [rd for rd in far if min(rd, NZ - rd) > 2]
     step = max(BATCH_AT, 1)
     batches = [(lo, min(lo + step, len(far))) for lo in range(0, len(far), step)]
 
@@ -118,10 +121,9 @@
     def sig(dev):
         pl.semaphore_signal(bar, inc=1, device_id=dev, device_id_type=MESH)
 
-    for d in range(1, NZ):
+    for d in far_first:
         sig(zdev(d))
         sig(zcross(d))
-    sig(partner)
 
     def bar_ep(i, carry):
         e = (me + i) % EP
@@ -130,6 +132,7 @@
         return carry
 
     lax.fori_loop(1, EP, bar_ep, 0, unroll=True)
+    sig(partner)
 
     loads = []
 
@@ -259,6 +262,7 @@
     conv_part = par(0) + sum(
         par(4 + j) * jnp.concatenate([conv_p[0, j], conv_p[1, j]], axis=1).astype(F32) for j in range(3)
     )
+    base_decay = 8.0 * log_sigmoid(par(3))
     loads[k_bw].wait()
     loads[k_gw].wait()
     take(x_bw, x_gw)
@@ -303,7 +307,7 @@
 
     recur_gate = sigmoid(block_map(rw_p) + par(1))
     input_gate = sigmoid(block_map(iw_p) + par(2))
-    log_decay = 8.0 * recur_gate * log_sigmoid(par(3))
+    log_decay = recur_gate * base_decay
     state = jnp.concatenate([state_p[0], state_p[1]], axis=1)
     new_state = jnp.exp(log_decay) * state + jnp.sqrt(expm1_neg(2.0 * log_decay)) * (input_gate * conv_out)
     hid_b[0] = (new_state * gelu(gating)).astype(BF16)
@@ -376,11 +380,6 @@
         half = mm(selh_v[...], resid[:, j * 128 : (j + 1) * 128]).astype(BF16)
         ysel[:, c if j == 0 else other] = half.reshape(EP, CAP, 128)
     dispatch(ysel, xown, s_d.at[0], r_d.at[0])
-    wait_blocks(xown, own_half, r_d.at[0])
-    for p in range(2):
-        xbuf[0, p * HS : (p + 1) * HS] = xown[0:HS, p] + xown[HS : 2 * HS, p]
-    for rd in sorted(near, key=lambda d: -min(d, NZ - d)):
-        send(xbuf.at[0], xbuf.at[rd], s_h.at[rd], r_h.at[rd], zdev(back_rel(rd)))
     for b, (lo, hi) in enumerate(batches):
         for n in range(lo, hi):
             rd = far[n]
@@ -391,6 +390,11 @@
         for n in range(lo, hi):
             yfar[:, n] = rows_out[:, (n - lo) * 128 : (n - lo + 1) * 128].reshape(EP, CAP, 128)
         dispatch(yfar, xfar, s_d.at[1 + b], r_d.at[1 + b], (lo, hi))
+    wait_blocks(xown, own_half, r_d.at[0])
+    for p in range(2):
+        xbuf[0, p * HS : (p + 1) * HS] = xown[0:HS, p] + xown[HS : 2 * HS, p]
+    for rd in near:
+        send(xbuf.at[0], xbuf.at[rd], s_h.at[rd], r_h.at[rd], zdev(back_rel(rd)))
     wait(res_c.at[0, other], r_c.at[0, 1])
     for rd in near:
         wait(res_c.at[rd, c], r_c.at[rd, 0])
@@ -421,10 +425,10 @@
     ss_tot = jnp.sum(ss_own[...] + ss_in[...], axis=1, keepdims=True)
     rstd2 = lax.rsqrt(ss_tot / WIDTH + EPS)
     logits = (lg_own[...] + lg_in[...]) * rstd2
-    e_exp = jnp.exp(logits[:, 0:L])
+    e_exp = jnp.where(selt_v[1] > 0.0, jnp.exp(logits[:, 0:L]), 0.0)
     g_exp = jnp.exp(logits[:, L : 2 * L])
-    e_den = jnp.sum(e_exp * selt_v[1], axis=1, keepdims=True) * (1.0 / CAP)
-    g_den = jnp.sum(g_exp, axis=1, keepdims=True) * (1.0 / (CAP * GS))
+    e_den = jnp.sum(e_exp * (1.0 / CAP), axis=1, keepdims=True)
+    g_den = jnp.sum(g_exp * (1.0 / (CAP * GS)), axis=1, keepdims=True)
     combine = selt_v[0] * (g_exp / g_den) * (e_exp / e_den)
     comb_hi = combine.astype(BF16)
     comb_lo = (combine - comb_hi.astype(F32)).astype(BF16)
@@ -627,7 +631,7 @@
     V = pltpu.VMEM
     dma = pltpu.SemaphoreType.DMA
     H = S // 2
-    near_count = len([d for d in range(1, NZ) if min(d, NZ - d) <= NEAR])
+    near_count = 3 if NZ > 4 else min(NZ - 1, 2)
     NF = max(NZ - 1 - near_count, 1)
     NFE = max(len([d for d in range(1, NZ) if min(d, NZ - d) > ENEAR]), 1)
     scratch = [

time: 49.4 us -> 49.3 us (level)
  no operation moved by 1% of the time
where the time goes in v6:
time: 49.3 us; the launch traced here: 49.2 us
  Pallas kernels  48.5 us (98%)
  between operations  0.65 us (1%)
    pallas_call x1, Pallas kernels, on_device(): pl.pallas_call(functools.partial(kernel, EP, NZ, S, CAP, GS), out_shape=(...  47.9 us

profile of v6, /device:TPU:1, one launch (start us, length us, event | category | flops | bytes accessed | tf_op | source)
XLA Modules:
  0.0 49.2 jit_solution(776548879702182220)
XLA Ops:
  0.6 47.9 %layer.1 = (bf16[64,128]{1,0:T(8,128)(2,1)S(1)}, f32[64,128]{1,0:T(8,128)S(1)}, bf16[3,64,128]{2,1,0:T(8,128)(2,1)S(1)}) custom-call(bf16[64,128]{1,0:T(8,128)(2,1)} %tok_h.1, bf16[3,64,128]{2,1,0:T(8,128)(2,1)} %bitcast.18, f32[64,128]{1,0:T(8,128)} %state_h.1, bf16[128]{0:T(256)(128)(2,1)} %n1_h.1, bf16[128]{0:T(256)(128)(2,1)} %n2_h.1, ...), custom_call_target="tpu_custom_call" | custom-call | tf_op jit(solution)/shard_map/layer/pallas_call | solution.py:705
  48.5 0.7 %emit.1 = (bf16[64,128]{1,0:T(8,128)(2,1)}, f32[64,128]{1,0:T(8,128)}, bf16[3,64,128]{2,1,0:T(8,128)(2,1)}) custom-call(bf16[64,128]{1,0:T(8,128)(2,1)S(1)} %get-tuple-element.9.a_v, f32[64,128]{1,0:T(8,128)S(1)} %get-tuple-element.10.b_v, bf16[3,64,128]{2,1,0:T(8,128)(2,1)S(1)} %get-tuple-element.11.c_v), custom_call_target="tpu_custom_call" | custom-call | tf_op jit(solution)/shard_map/emit/pallas_call | solution.py:722

commit v7 on v6

--- a/solution.py
+++ b/solution.py
@@ -288,6 +288,8 @@
             x = tok_a[rd, j].astype(F32)
             sums[0] = sums[0] + x * x
             parts.append((x * gain_a[rd, j][0:1, :]).astype(BF16))
+        if rd == near_first[-1]:
+            x_ow = share(ow_h, ow_p.at[1])
         xg = jnp.concatenate(parts, axis=1)
         sums[1] = sums[1] + mm(xg, both(bw_p, rd))
         sums[2] = sums[2] + mm(xg, both(gw_p, rd))
@@ -319,10 +321,8 @@
     ns_x[...] = new_state[:, 128:256]
     branch_v[my_rows, :] = branch[:, 0:128]
     br_x[...] = branch[:, 128:256]
-    send_down([d for d in far_first if min(d, NZ - d) in (1, 2)])
     send(ns_x, nstate_v.at[my_rows], s_o.at[0], r_o.at[0], partner)
     send(br_x, branch_v.at[my_rows], s_o.at[1], r_o.at[1], partner)
-    x_ow = share(ow_h, ow_p.at[1])
     loads[k_convo].wait()
     nconv_o[0:2] = conv_v[...]
     loads[k_ow].wait()
@@ -412,9 +412,7 @@
     ss_own[...] = ss_row
     send(lg_own, lg_in, s_l.at[0], r_l.at[0], partner)
     send(ss_own, ss_in, s_l.at[1], r_l.at[1], partner)
-    for rd in e_near:
-        wait(wdn.at[rd, 0], r_w.at[rd, 0])
-        send(wdn.at[rd, 0], wdn.at[rd, 1], f_w.at[rd], r_w.at[rd, 1], partner)
+    send_down([d for d in far_first if min(d, NZ - d) in (1, 2)])
     wait(ns_x, r_o.at[0])
     wait(br_x, r_o.at[1])
     nstate_o[...] = nstate_v[...]
@@ -512,6 +510,9 @@
         put(yf_v, mm(hid_e[0], own_down(d)), (n,))
     if e_far:
         give_back(yf_v, backf_v, s_k, r_k.at[0])
+    for rd in e_near:
+        wait(wdn.at[rd, 0], r_w.at[rd, 0])
+        send(wdn.at[rd, 0], wdn.at[rd, 1], f_w.at[rd], r_w.at[rd, 1], partner)
     out = mm(hid_e[0], own_down(0))
     for rd in e_near:
         wait(wdn.at[rd, 1], r_w.at[rd, 1])

time: 49.3 us -> 48.8 us (0.990)
  Pallas kernels: 48.5 us -> 48 us
    pallas_call x1, Pallas kernels: 47.9 us -> 47.3 us  [on_device(): pl.pallas_call(functools.partial(kernel, EP, NZ, S, CAP, GS), out_shape=(...]
where the time goes in v7:
time: 48.8 us; the launch traced here: 48.7 us
  Pallas kernels  48 us (98%)
  between operations  0.65 us (1%)
    pallas_call x1, Pallas kernels, on_device(): pl.pallas_call(functools.partial(kernel, EP, NZ, S, CAP, GS), out_shape=(...  47.3 us

profile of v7, /device:TPU:1, one launch (start us, length us, event | category | flops | bytes accessed | tf_op | source)
XLA Modules:
  0.0 48.7 jit_solution(9808861173664902247)
XLA Ops:
  0.6 47.3 %layer.1 = (bf16[64,128]{1,0:T(8,128)(2,1)S(1)}, f32[64,128]{1,0:T(8,128)S(1)}, bf16[3,64,128]{2,1,0:T(8,128)(2,1)S(1)}) custom-call(bf16[64,128]{1,0:T(8,128)(2,1)} %tok_h.1, bf16[3,64,128]{2,1,0:T(8,128)(2,1)} %bitcast.18, f32[64,128]{1,0:T(8,128)} %state_h.1, bf16[128]{0:T(256)(128)(2,1)} %n1_h.1, bf16[128]{0:T(256)(128)(2,1)} %n2_h.1, ...), custom_call_target="tpu_custom_call" | custom-call | tf_op jit(solution)/shard_map/layer/pallas_call | solution.py:706
  48.0 0.7 %emit.1 = (bf16[64,128]{1,0:T(8,128)(2,1)}, f32[64,128]{1,0:T(8,128)}, bf16[3,64,128]{2,1,0:T(8,128)(2,1)}) custom-call(bf16[64,128]{1,0:T(8,128)(2,1)S(1)} %get-tuple-element.9.a_v, f32[64,128]{1,0:T(8,128)S(1)} %get-tuple-element.10.b_v, bf16[3,64,128]{2,1,0:T(8,128)(2,1)S(1)} %get-tuple-element.11.c_v), custom_call_target="tpu_custom_call" | custom-call | tf_op jit(solution)/shard_map/emit/pallas_call | solution.py:723
